TPU v7x, 128 devices: a whole 4x4x4 slice. The times are simulated.
128 devices in a mesh: kv: 16 (over z, y), tp: 8 (over x, core).
Axes of the slice: x: 4, y: 4, z: 4, core: 2. Of those that a mesh axis runs over, the one named last changes fastest.
Arguments:
- activations: bfloat16 [128, 4096], P(None, ('kv', 'tp')), may hold values from -60 to 60
- mixer_gain: bfloat16 [4096], P(('kv', 'tp')), may hold values from 0.099609375 to 1.8984375
- channel_gain: bfloat16 [4096], P(('kv', 'tp')), may hold values from 0.099609375 to 1.8984375
- query_weight: bfloat16 [4096, 4096], P('kv', 'tp'), may hold values from -0.09375 to 0.09375
- key_weight: bfloat16 [4096, 4096], P('kv', 'tp'), may hold values from -0.09375 to 0.09375
- value_weight: bfloat16 [4096, 8192], P('kv', 'tp'), may hold values from -0.09375 to 0.09375
- gate_weight: bfloat16 [4096, 8192], P('kv', 'tp'), may hold values from -0.09375 to 0.09375
- output_weight: bfloat16 [8192, 4096], P('tp', 'kv'), may hold values from -0.1875 to 0.1875
- up_weight: bfloat16 [4096, 16384], P('kv', 'tp'), may hold values from -0.09375 to 0.09375
- down_weight: bfloat16 [16384, 4096], P('tp', 'kv'), may hold values from -0.046875 to 0.046875
- state_in: float32 [128, 16, 256, 512], P('kv', 'tp'), may hold values from -0.5 to 0.5
Outputs:
- activations_out: bfloat16 [128, 4096], P(None, ('kv', 'tp'))
- state_out: float32 [128, 16, 256, 512], P('kv', 'tp')
All inputs are finite; a program needn't handle non-finite values.
Results may differ from a plain program's by a relative error of at most 0.022.
Values may be sent and summed in bfloat16 or wider, within the bound.
No kernel may reach another device: no remote copies, remote signals or barrier semaphores. Data moves between devices by JAX's collectives and lax.ppermute only.
A program may use at most 64 MiB of HBM per device.

v0:
```python
import jax
import jax.numpy as jnp
from jax import lax
from jax.sharding import PartitionSpec as P

D = 4096
HEADS = 16
DK = 256
DV = 512


EPS = 1e-06


def sent_to_all(value, axis):
    size = lax.axis_size(axis)
    return lax.all_to_all(
        jnp.broadcast_to(value[None], (size, *value.shape)), axis, 0, 0, tiled=True
    )


def in_order(parts, dim):
    parts = jnp.moveaxis(parts, 0, dim)
    dims = parts.shape
    return parts.reshape(*dims[:dim], dims[dim] * dims[dim + 1], *dims[dim + 2 :])


def collect(value, axis, dim):
    parts = sent_to_all(value, axis)
    return in_order(parts, dim)


def split_up(value, dim, size):
    before, after = (value.shape[:dim], value.shape[dim + 1 :])
    return jnp.moveaxis(value.reshape(*before, size, -1, *after), dim, 0)


def sum_at_owner(value, axis, dim):
    size = lax.axis_size(axis)
    parts = lax.all_to_all(split_up(value, dim, size), axis, 0, 0, tiled=True)
    return jnp.sum(parts.astype(jnp.float32), axis=0)


def side_by_side(arrays, axis, dim, along):
    both = jnp.concatenate(arrays, axis=along)
    filled, at, gathered = (sum_at_owner(both, axis, dim), 0, [])
    for a in arrays:
        gathered.append(lax.slice_in_dim(filled, at, at + a.shape[along], axis=along))
        at += a.shape[along]
    return tuple(gathered)


def head_decays(count):
    index = jnp.arange(count, dtype=jnp.float32)
    return 1.0 - 2.0 ** (-1.0 - 6.0 * index / (count - 1))


def select_rows(values, groups):
    shaped = values.reshape((groups, -1) + values.shape[1:])
    return shaped.reshape((-1,) + values.shape[1:])


def retain(query_sum, key_sum, value_sum, gate_sum, scale_rows, old_state, rates):
    count, heads = (old_state.shape[0], old_state.shape[1])
    query = (scale_rows * query_sum).reshape(count, heads, DK)
    key = (scale_rows * key_sum * DK ** (-0.5)).reshape(count, heads, DK)
    value = (scale_rows * value_sum).reshape(count, heads, DV)
    gate = scale_rows * gate_sum
    new_state = rates[None, :, None, None] * old_state + key[:, :, :, None] * value[:, :, None, :]
    output = jnp.einsum("shd,shde->she", query, new_state, precision=lax.Precision.HIGHEST)
    output = output * lax.rsqrt(jnp.mean(output * output, axis=2, keepdims=True) + EPS)
    mixed = (jax.nn.silu(gate) * output.reshape(count, heads * DV)).astype(jnp.bfloat16)
    return (new_state, mixed)


def per_device(
    activations,
    mixer_gain,
    channel_gain,
    query_weight,
    key_weight,
    value_weight,
    gate_weight,
    output_weight,
    up_weight,
    down_weight,
    state_in,
):
    groups = lax.axis_size("kv")
    heads_dev = state_in.shape[1]
    rates = lax.dynamic_slice_in_dim(
        head_decays(HEADS), lax.axis_index("tp") * heads_dev, heads_dev, 0
    )
    stream = activations.astype(jnp.float32)
    squares = jnp.sum(stream * stream, axis=1, keepdims=True)
    normed = (stream * mixer_gain.astype(jnp.float32)).astype(jnp.bfloat16)
    block, square_cols = (
        collect(normed, "tp", 1),
        collect(squares.astype(jnp.bfloat16), "tp", 1).astype(squares.dtype),
    )
    block_squares = jnp.sum(square_cols, axis=1, keepdims=True)
    rows = select_rows(block, groups)
    query_term = jnp.dot(rows, query_weight, preferred_element_type=jnp.float32)
    key_term = jnp.dot(rows, key_weight, preferred_element_type=jnp.float32)
    value_term = jnp.dot(rows, value_weight, preferred_element_type=jnp.float32)
    gate_term = jnp.dot(rows, gate_weight, preferred_element_type=jnp.float32)
    query_sum, key_sum, value_sum, gate_sum, piece_totals = side_by_side(
        (
            query_term.astype(jnp.bfloat16),
            key_term.astype(jnp.bfloat16),
            value_term.astype(jnp.bfloat16),
            gate_term.astype(jnp.bfloat16),
            select_rows(block_squares, groups).astype(jnp.bfloat16),
        ),
        "kv",
        0,
        1,
    )
    scale_rows = lax.rsqrt(piece_totals / D + EPS)
    new_state, mixed = retain(query_sum, key_sum, value_sum, gate_sum, scale_rows, state_in, rates)
    out_terms = jnp.dot(collect(mixed, "kv", 0), output_weight, preferred_element_type=jnp.float32)
    attention = sum_at_owner(out_terms.astype(jnp.bfloat16), "tp", 1)
    middle = (stream + attention).astype(jnp.bfloat16)
    middle = lax.optimization_barrier(middle).astype(jnp.float32)
    middle_squares = jnp.sum(middle * middle, axis=1, keepdims=True)
    channel_normed = (middle * channel_gain.astype(jnp.float32)).astype(jnp.bfloat16)
    channel_block, channel_cols = (
        collect(channel_normed, "tp", 1),
        collect(middle_squares.astype(jnp.bfloat16), "tp", 1).astype(middle_squares.dtype),
    )
    up_sum, own_channel = side_by_side(
        (
            jnp.dot(channel_block, up_weight, preferred_element_type=jnp.float32).astype(
                jnp.bfloat16
            ),
            jnp.sum(channel_cols, axis=1, keepdims=True).astype(jnp.bfloat16),
        ),
        "kv",
        0,
        1,
    )
    lifted = lax.rsqrt(own_channel / D + EPS) * up_sum
    hidden = jnp.square(jax.nn.relu(lifted)).astype(jnp.bfloat16)
    down_terms = jnp.dot(collect(hidden, "kv", 0), down_weight, preferred_element_type=jnp.float32)
    lowered = sum_at_owner(down_terms.astype(jnp.bfloat16), "tp", 1)
    return ((middle + lowered).astype(jnp.bfloat16), new_state)


def solution(mesh):
    return jax.shard_map(
        per_device,
        mesh=mesh,
        in_specs=(
            P(None, ("kv", "tp")),
            P(("kv", "tp")),
            P(("kv", "tp")),
            P("kv", "tp"),
            P("kv", "tp"),
            P("kv", "tp"),
            P("kv", "tp"),
            P("tp", "kv"),
            P("kv", "tp"),
            P("tp", "kv"),
            P("kv", "tp", None, None),
        ),
        out_specs=(P(None, ("kv", "tp")), P("kv", "tp", None, None)),
        check_vma=False,
    )
```

profile of v0, /device:TPU:1, one launch (start us, length us, event | category | flops | bytes accessed | tf_op | source)
XLA Modules:
  0.0 141.7 jit_solution(3297570347268671122)
XLA Ops:
  0.6 0.0 copy-start
  0.6 0.7 convert_element_type.112
  1.4 0.8 fusion.16
  2.2 10.2 %all_to_all.50 = bf16[8,128,1]{1,2,0:T(2,128)(2,1)S(1)} all-to-all(bf16[8,128,1]{1,2,0:T(2,128)(2,1)S(1)} %broadcast_in_dim.13), channel_id=1, replica_groups=mesh['kv'=16,'tp'=8] {'tp'}, dimensions={0} | all-to-all | bytes 4096 | tf_op jit(solution)/shard_map/all_to_all | solution.py:17
  12.4 0.6 broadcast_in_dim.12
  13.0 3.9 %all-to-all-start = ((bf16[8,128,32]{1,2,0:T(8,128)(2,1)}), bf16[8,128,32]{1,2,0:T(8,128)(2,1)S(1)}, u32[]{:S(2)}, u32[]{:S(2)}) async-start(bf16[8,128,32]{1,2,0:T(8,128)(2,1)} %broadcast_in_dim.12), calls=%async_computation | async-start | bytes 131072 | tf_op jit(solution)/shard_map/all_to_all | solution.py:17
  17.0 0.2 convert_element_type.136
  17.2 4.6 %all-to-all-done = bf16[8,128,32]{1,2,0:T(8,128)(2,1)S(1)} async-done(((bf16[8,128,32]{1,2,0:T(8,128)(2,1)}), bf16[8,128,32]{1,2,0:T(8,128)(2,1)S(1)}, u32[]{:S(2)}, u32[]{:S(2)}) %all-to-all-start) | async-done | bytes 65568 | tf_op jit(solution)/shard_map/all_to_all | solution.py:17
  21.8 1.8 %fusion.6 = bf16[16,8,3073]{2,1,0:T(8,128)(2,1)} fusion(bf16[128,256]{0,1:T(8,128)(2,1)S(1)} %bitcast.60, bf16[256,512]{1,0:T(8,128)(2,1)} %param.14), kind=kOutput, calls=%fused_computation.13 | convolution fusion | flops 33619968 | bytes 458752 | tf_op jit(solution)/shard_map/dot_general | solution.py:103
  23.6 1.8 %fusion.8 = bf16[16,8,3073]{2,1,0:T(8,128)(2,1)} fusion(bf16[16,8,3073]{2,1,0:T(8,128)(2,1)} %fusion.6, bf16[128,256]{0,1:T(8,128)(2,1)S(1)} %bitcast.61, bf16[256,512]{1,0:T(8,128)(2,1)} %param.15), kind=kOutput, calls=%fused_computation.15 | convolution fusion | flops 33619968 | bytes 458752 | tf_op jit(solution)/shard_map/dot_general | solution.py:104
  25.4 2.0 %fusion.2 = bf16[16,8,3073]{2,1,0:T(8,128)(2,1)} fusion(bf16[16,8,3073]{2,1,0:T(8,128)(2,1)} %fusion.8, bf16[128,256]{0,1:T(8,128)(2,1)S(1)} %bitcast.62, bf16[256,1024]{1,0:T(8,128)(2,1)} %param.16), kind=kOutput, calls=%fused_computation.7 | convolution fusion | flops 67239936 | bytes 851968 | tf_op jit(solution)/shard_map/dot_general | solution.py:105
  27.4 2.0 %fusion.4 = bf16[16,8,3073]{2,1,0:T(8,128)(2,1)} fusion(bf16[16,8,3073]{2,1,0:T(8,128)(2,1)} %fusion.2, bf16[128,256]{0,1:T(8,128)(2,1)S(1)} %bitcast.63, bf16[256,1024]{1,0:T(8,128)(2,1)} %param.17), kind=kOutput, calls=%fused_computation.9 | convolution fusion | flops 67239936 | bytes 851968 | tf_op jit(solution)/shard_map/dot_general | solution.py:106
  29.4 0.6 constant_dynamic-update-slice_fusion
  30.1 7.8 %all-to-all-start.2 = ((bf16[16,8,3073]{2,1,0:T(8,128)(2,1)}), bf16[16,8,3073]{2,1,0:T(8,128)(2,1)S(1)}, u32[]{:S(2)}, u32[]{:S(2)}) async-start(bf16[16,8,3073]{2,1,0:T(8,128)(2,1)} %constant_dynamic-update-slice_fusion), calls=%async_computation.2 | async-start | bytes 1638400 | tf_op jit(solution)/shard_map/all_to_all | solution.py:40
  37.9 0.1 dynamic_slice.3
  37.9 13.4 %all-to-all-done.2 = bf16[16,8,3073]{2,1,0:T(8,128)(2,1)S(1)} async-done(((bf16[16,8,3073]{2,1,0:T(8,128)(2,1)}), bf16[16,8,3073]{2,1,0:T(8,128)(2,1)S(1)}, u32[]{:S(2)}, u32[]{:S(2)}) %all-to-all-start.2) | async-done | bytes 786720 | tf_op jit(solution)/shard_map/all_to_all | solution.py:40
  51.3 0.1 convert_reduce_fusion
  51.4 0.1 fusion.29
  51.6 0.1 slice_multiply_fusion.1
  51.6 0.1 slice_multiply_fusion.4
  51.8 4.1 %multiply_add_fusion = f32[8,2,256,512]{3,2,1,0:T(8,128)S(1)} fusion(f32[8,2,256,512]{3,2,1,0:T(8,128)} %param.21, f32[8,2,512]{2,1,0:T(2,128)S(1)} %copy.37, f32[8,2,256]{2,1,0:T(2,128)S(1)} %copy.36, f32[2]{0:T(128)S(1)} %dynamic_slice.3), kind=kLoop, calls=%fused_computation | loop fusion | flops 6291456 | bytes 16826376 | tf_op jit(solution)/shard_map/add | solution.py:69
  55.9 0.0 copy-start.5
  55.9 3.4 %copy-done.1 = f32[8,2,256,512]{3,2,1,0:T(8,128)} copy-done((f32[8,2,256,512]{3,2,1,0:T(8,128)}, f32[8,2,256,512]{3,2,1,0:T(8,128)S(1)}, u32[]{:S(2)}) %copy-start.1) | copy-done | bytes 8388632
  59.3 4.1 %fusion.22 = f32[8,2,1,512]{3,2,1,0:T(1,128)S(1)} fusion(f32[8,2,256,512]{3,2,1,0:T(8,128)S(1)} %multiply_add_fusion, f32[8,2,256,1]{2,0,1,3:T(8,128)S(1)} %bitcast.68), kind=kOutput, calls=%fused_computation.49 | convolution fusion | flops 25165824 | bytes 8437760 | tf_op jit(solution)/shard_map/shd,shde->she/dot_general | solution.py:70
  63.3 0.1 fusion.14
  63.4 0.1 bitcast_multiply_fusion
  63.5 0.1 multiply_convert_fusion
  63.6 11.4 %all_to_all.51 = bf16[16,8,1024]{2,1,0:T(8,128)(2,1)S(1)} all-to-all(bf16[16,8,1024]{2,1,0:T(8,128)(2,1)S(1)} %broadcast_in_dim.14), channel_id=1, replica_groups=mesh['kv'=16,'tp'=8] {'kv'}, dimensions={0} | all-to-all | bytes 524288 | tf_op jit(solution)/shard_map/all_to_all | solution.py:17
  75.0 0.2 convolution_convert_fusion.6
  75.2 0.7 copy.38
  75.9 5.6 %all-to-all-start.4 = ((bf16[8,128,32]{1,2,0:T(8,128)(2,1)}), bf16[8,128,32]{1,2,0:T(8,128)(2,1)S(1)}, u32[]{:S(2)}, u32[]{:S(2)}) async-start(bf16[8,128,32]{1,2,0:T(8,128)(2,1)} %bitcast.15), calls=%async_computation.4 | async-start | bytes 131072 | tf_op jit(solution)/shard_map/all_to_all | solution.py:40
  81.5 4.9 %all-to-all-done.4 = bf16[8,128,32]{1,2,0:T(8,128)(2,1)S(1)} async-done(((bf16[8,128,32]{1,2,0:T(8,128)(2,1)}), bf16[8,128,32]{1,2,0:T(8,128)(2,1)S(1)}, u32[]{:S(2)}, u32[]{:S(2)}) %all-to-all-start.4) | async-done | bytes 65568 | tf_op jit(solution)/shard_map/all_to_all | solution.py:40
  86.4 0.1 fusion.18
  86.5 7.7 %all_to_all.52 = bf16[8,128,1]{1,2,0:T(2,128)(2,1)S(1)} all-to-all(bf16[8,128,1]{1,2,0:T(2,128)(2,1)S(1)} %broadcast_in_dim.16), channel_id=1, replica_groups=mesh['kv'=16,'tp'=8] {'tp'}, dimensions={0} | all-to-all | bytes 4096 | tf_op jit(solution)/shard_map/all_to_all | solution.py:17
  94.2 0.6 broadcast_in_dim.15
  94.8 3.9 %all-to-all-start.5 = ((bf16[8,128,32]{1,2,0:T(8,128)(2,1)}), bf16[8,128,32]{1,2,0:T(8,128)(2,1)S(1)}, u32[]{:S(2)}, u32[]{:S(2)}) async-start(bf16[8,128,32]{1,2,0:T(8,128)(2,1)} %broadcast_in_dim.15), calls=%async_computation.5 | async-start | bytes 131072 | tf_op jit(solution)/shard_map/all_to_all | solution.py:17
  98.8 0.2 convert_element_type.137
  99.1 4.6 %all-to-all-done.5 = bf16[8,128,32]{1,2,0:T(8,128)(2,1)S(1)} async-done(((bf16[8,128,32]{1,2,0:T(8,128)(2,1)}), bf16[8,128,32]{1,2,0:T(8,128)(2,1)S(1)}, u32[]{:S(2)}, u32[]{:S(2)}) %all-to-all-start.5) | async-done | bytes 65568 | tf_op jit(solution)/shard_map/all_to_all | solution.py:17
  103.7 0.3 fusion
  104.1 13.7 %all_to_all.53 = bf16[16,8,2049]{2,1,0:T(8,128)(2,1)S(1)} all-to-all(bf16[16,8,2049]{2,1,0:T(8,128)(2,1)S(1)} %pad_maximum_fusion), channel_id=1, replica_groups=mesh['kv'=16,'tp'=8] {'kv'}, dimensions={0} | all-to-all | bytes 1049088 | tf_op jit(solution)/shard_map/all_to_all | solution.py:40
  117.8 0.1 convert_reduce_fusion.1
  117.9 0.1 fusion.26
  118.0 0.1 fusion.13
  118.1 12.2 %all_to_all.54 = bf16[16,8,2048]{2,1,0:T(8,128)(2,1)S(1)} all-to-all(bf16[16,8,2048]{2,1,0:T(8,128)(2,1)S(1)} %broadcast_in_dim.17), channel_id=1, replica_groups=mesh['kv'=16,'tp'=8] {'kv'}, dimensions={0} | all-to-all | bytes 1048576 | tf_op jit(solution)/shard_map/all_to_all | solution.py:17
  130.4 0.3 convolution_convert_fusion.5
  130.7 0.1 copy.40
  130.8 10.3 %all_to_all.55 = bf16[8,128,32]{1,2,0:T(8,128)(2,1)S(1)} all-to-all(bf16[8,128,32]{1,2,0:T(8,128)(2,1)S(1)} %bitcast.65), channel_id=1, replica_groups=mesh['kv'=16,'tp'=8] {'tp'}, dimensions={0} | all-to-all | bytes 131072 | tf_op jit(solution)/shard_map/all_to_all | solution.py:40
  141.1 0.6 fusion.20
  (24 shorter events, 0.3 us)
Async XLA Ops:
  0.6 103.0 %copy-start = (bf16[256,2048]{1,0:T(8,128)(2,1)S(1)}, bf16[256,2048]{1,0:T(8,128)(2,1)}, u32[]{:S(2)}) copy-start(bf16[256,2048]{1,0:T(8,128)(2,1)} %param.19) | copy-start | bytes 3145732
  13.0 8.8 %all-to-all-start = ((bf16[8,128,32]{1,2,0:T(8,128)(2,1)}), bf16[8,128,32]{1,2,0:T(8,128)(2,1)S(1)}, u32[]{:S(2)}, u32[]{:S(2)}) async-start(bf16[8,128,32]{1,2,0:T(8,128)(2,1)} %broadcast_in_dim.12), calls=%async_computation | async-start | bytes 131072 | tf_op jit(solution)/shard_map/all_to_all | solution.py:17
  30.1 21.3 %all-to-all-start.2 = ((bf16[16,8,3073]{2,1,0:T(8,128)(2,1)}), bf16[16,8,3073]{2,1,0:T(8,128)(2,1)S(1)}, u32[]{:S(2)}, u32[]{:S(2)}) async-start(bf16[16,8,3073]{2,1,0:T(8,128)(2,1)} %constant_dynamic-update-slice_fusion), calls=%async_computation.2 | async-start | bytes 1638400 | tf_op jit(solution)/shard_map/all_to_all | solution.py:40
  55.9 3.4 %copy-start.1 = (f32[8,2,256,512]{3,2,1,0:T(8,128)}, f32[8,2,256,512]{3,2,1,0:T(8,128)S(1)}, u32[]{:S(2)}) copy-start(f32[8,2,256,512]{3,2,1,0:T(8,128)S(1)} %multiply_add_fusion) | copy-start | bytes 25165828
  55.9 19.1 %copy-start.3 = (bf16[1024,256]{1,0:T(8,128)(2,1)S(1)}, bf16[1024,256]{1,0:T(8,128)(2,1)}, u32[]{:S(2)}) copy-start(bf16[1024,256]{1,0:T(8,128)(2,1)} %param.18) | copy-start | bytes 1572868
  55.9 25.6 %copy-start.5 = (bf16[32]{0:T(256)(128)(2,1)S(1)}, bf16[32]{0:T(256)(128)(2,1)}, u32[]{:S(2)}) copy-start(bf16[32]{0:T(256)(128)(2,1)} %param.13) | copy-start | bytes 196
  55.9 30.5 %copy-start.4 = (bf16[128,32]{0,1:T(8,128)(2,1)S(1)}, bf16[128,32]{0,1:T(8,128)(2,1)}, u32[]{:S(2)}) copy-start(bf16[128,32]{0,1:T(8,128)(2,1)} %param.11) | copy-start | bytes 24580
  59.3 71.1 %copy-start.2 = (bf16[2048,256]{1,0:T(8,128)(2,1)S(1)}, bf16[2048,256]{1,0:T(8,128)(2,1)}, u32[]{:S(2)}) copy-start(bf16[2048,256]{1,0:T(8,128)(2,1)} %param.20) | copy-start | bytes 3145732
  75.9 10.4 %all-to-all-start.4 = ((bf16[8,128,32]{1,2,0:T(8,128)(2,1)}), bf16[8,128,32]{1,2,0:T(8,128)(2,1)S(1)}, u32[]{:S(2)}, u32[]{:S(2)}) async-start(bf16[8,128,32]{1,2,0:T(8,128)(2,1)} %bitcast.15), calls=%async_computation.4 | async-start | bytes 131072 | tf_op jit(solution)/shard_map/all_to_all | solution.py:40
  94.8 8.8 %all-to-all-start.5 = ((bf16[8,128,32]{1,2,0:T(8,128)(2,1)}), bf16[8,128,32]{1,2,0:T(8,128)(2,1)S(1)}, u32[]{:S(2)}, u32[]{:S(2)}) async-start(bf16[8,128,32]{1,2,0:T(8,128)(2,1)} %broadcast_in_dim.15), calls=%async_computation.5 | async-start | bytes 131072 | tf_op jit(solution)/shard_map/all_to_all | solution.py:17
where the time goes:
time: 143 us; the launch traced here: 142 us
  blocking collectives  65.5 us (46%)
  waiting for transfers between devices  27.5 us (19%)
  starting transfers between devices  21.2 us (15%)
  matrix products  12.6 us (9%)
  other arithmetic  7.36 us (5%)
  local copies, waits for them, and re-layouts  6.76 us (5%)
    all_to_all x4, blocking collectives, sent_to_all(): lax.all_to_all(jnp.broadcast_to(value[None], (size, *value.shape)), axis,...  41.5 us
    all_to_all x2, blocking collectives, sum_at_owner(): parts = lax.all_to_all(split_up(value, dim, size), axis, 0, 0, tiled=True)  24 us
    all_to_all x2, waiting for transfers between devices, sum_at_owner(): parts = lax.all_to_all(split_up(value, dim, size), axis, 0, 0, tiled=True)  18.2 us
    all_to_all x2, starting transfers between devices, sum_at_owner(): parts = lax.all_to_all(split_up(value, dim, size), axis, 0, 0, tiled=True)  13.3 us
    all_to_all x2, waiting for transfers between devices, sent_to_all(): lax.all_to_all(jnp.broadcast_to(value[None], (size, *value.shape)), axis,...  9.22 us
    all_to_all x2, starting transfers between devices, sent_to_all(): lax.all_to_all(jnp.broadcast_to(value[None], (size, *value.shape)), axis,...  7.89 us
    add x1, other arithmetic, retain(): rates[None, :, None, None] * old_state  4.08 us
    dot_general x1, matrix products, retain(): jnp.einsum('shd,shde->she', query, new_state, precision=lax.Precision.HIG...  4.05 us
  transfers between devices with their start and end apart: 4, of which 4 were waited for; matrix products, arithmetic and copies ran while one was open for 0% of the time, Pallas kernels for 0%

commit v1 on v0

v1 whole, which is shorter than its diff:
```python
import jax
import jax.numpy as jnp
from jax import lax
from jax.sharding import PartitionSpec as P

D = 4096
HEADS = 16
DK = 256
DV = 512
EPS = 1e-06
F32 = jnp.float32
BF16 = jnp.bfloat16


def head_decays(count):
    index = jnp.arange(count, dtype=F32)
    return 1.0 - 2.0 ** (-1.0 - 6.0 * index / (count - 1))


def gather_all(value, axis):
    size = lax.axis_size(axis)
    return lax.all_to_all(
        jnp.broadcast_to(value[None], (size, *value.shape)), axis, 0, 0, tiled=True
    )


def spread_sum(value, axis):
    parts = lax.all_to_all(value, axis, 0, 0, tiled=True)
    return jnp.sum(parts.astype(F32), axis=0)


def swap_cores(value):
    return lax.ppermute(value, "tp", [(i, i ^ 1) for i in range(8)])


def shift_chips(value, step):
    return lax.ppermute(value, "tp", [(i, (i + 2 * step) % 8) for i in range(8)])


def retain(query_sum, key_sum, value_sum, gate_sum, scale_rows, old_state, rates):
    count, heads = (old_state.shape[0], old_state.shape[1])
    query = (scale_rows * query_sum).reshape(count, heads, DK)
    key = (scale_rows * key_sum * DK ** (-0.5)).reshape(count, heads, DK)
    value = (scale_rows * value_sum).reshape(count, heads, DV)
    gate = scale_rows * gate_sum
    new_state = rates[None, :, None, None] * old_state + key[:, :, :, None] * value[:, :, None, :]
    output = jnp.einsum("shd,shde->she", query, new_state, precision=lax.Precision.HIGHEST)
    output = output * lax.rsqrt(jnp.mean(output * output, axis=2, keepdims=True) + EPS)
    mixed = (jax.nn.silu(gate) * output.reshape(count, heads * DV)).astype(BF16)
    return (new_state, mixed)


def per_device(
    activations,
    mixer_gain,
    channel_gain,
    query_weight,
    key_weight,
    value_weight,
    gate_weight,
    output_weight,
    up_weight,
    down_weight,
    state_in,
):
    tp = lax.axis_index("tp")
    core = tp % 2
    chip = tp // 2
    heads_dev = state_in.shape[1]
    rates = lax.dynamic_slice_in_dim(head_decays(HEADS), tp * heads_dev, heads_dev, 0)

    rows = jnp.concatenate(
        [
            activations.T,
            jnp.pad(mixer_gain[None], ((0, 0), (0, 96))),
            jnp.pad(channel_gain[None], ((0, 6), (0, 96))),
        ],
        axis=0,
    )
    packed = gather_all(rows, "tp")
    stream = packed[:, :32].reshape(256, 128).T.astype(F32)
    mixer = packed[:, 32, :32].reshape(1, 256).astype(F32)
    channel = packed[:, 33, :32].reshape(1, 256).astype(F32)

    squares = jnp.sum(stream * stream, axis=1, keepdims=True)
    normed = (stream * mixer).astype(BF16)
    terms = [
        jnp.dot(normed, w, preferred_element_type=F32).astype(BF16)
        for w in (query_weight, key_weight, value_weight, gate_weight)
    ]
    terms.append(jnp.pad(squares.astype(BF16), ((0, 0), (0, 127))))
    sums = spread_sum(jnp.concatenate(terms, axis=1).reshape(16, 8, -1), "kv")
    scale_rows = lax.rsqrt(sums[:, 3072:3073] / D + EPS)
    new_state, mixed = retain(
        sums[:, :512], sums[:, 512:1024], sums[:, 1024:2048], sums[:, 2048:3072],
        scale_rows, state_in, rates,
    )

    mixed_all = gather_all(mixed, "kv").reshape(128, 1024)
    out_terms = jnp.dot(mixed_all, output_weight, preferred_element_type=F32).astype(BF16)
    halves = (out_terms[:, :128], out_terms[:, 128:])
    mine = jnp.where(core == 0, halves[0], halves[1])
    theirs = jnp.where(core == 0, halves[1], halves[0])
    pair = (mine.astype(F32) + swap_cores(theirs).astype(F32)).astype(BF16)
    attention = pair.astype(F32)
    for step in (1, 3, 2):
        attention = attention + shift_chips(pair, step).astype(F32)
    stream_half = jnp.where(core == 0, stream[:, :128], stream[:, 128:])
    middle_half = (stream_half + attention).astype(BF16)
    other_half = swap_cores(middle_half)
    middle_bf = jnp.concatenate(
        [
            jnp.where(core == 0, middle_half, other_half),
            jnp.where(core == 0, other_half, middle_half),
        ],
        axis=1,
    )
    middle = middle_bf.astype(F32)
    middle_squares = jnp.sum(middle * middle, axis=1, keepdims=True)
    channel_normed = (middle * channel).astype(BF16)
    up_terms = jnp.concatenate(
        [
            jnp.dot(channel_normed, up_weight, preferred_element_type=F32).astype(BF16),
            jnp.pad(middle_squares.astype(BF16), ((0, 0), (0, 127))),
        ],
        axis=1,
    )
    up_sum = spread_sum(up_terms.reshape(16, 8, -1), "kv")
    lifted = lax.rsqrt(up_sum[:, 2048:2049] / D + EPS) * up_sum[:, :2048]
    hidden = jnp.square(jax.nn.relu(lifted)).astype(BF16)

    hidden_all = gather_all(hidden, "kv").reshape(128, 2048)
    down_terms = jnp.dot(hidden_all, down_weight, preferred_element_type=F32).astype(BF16)
    down_t = down_terms.T.reshape(4, 2, 32, 128)
    mine = jnp.where(core == 0, down_t[:, 0], down_t[:, 1])
    theirs = jnp.where(core == 0, down_t[:, 1], down_t[:, 0])
    pair = (mine.astype(F32) + swap_cores(theirs).astype(F32)).astype(BF16)
    lowered = lax.dynamic_index_in_dim(pair, chip, 0, keepdims=False).astype(F32)
    for step in (1, 3, 2):
        piece = lax.dynamic_index_in_dim(pair, (chip + step) % 4, 0, keepdims=False)
        lowered = lowered + shift_chips(piece, step).astype(F32)
    own = lax.dynamic_slice_in_dim(middle_bf.T, tp * 32, 32, 0).astype(F32)
    return ((own + lowered).astype(BF16).T, new_state)


def solution(mesh):
    return jax.shard_map(
        per_device,
        mesh=mesh,
        in_specs=(
            P(None, ("kv", "tp")),
            P(("kv", "tp")),
            P(("kv", "tp")),
            P("kv", "tp"),
            P("kv", "tp"),
            P("kv", "tp"),
            P("kv", "tp"),
            P("tp", "kv"),
            P("kv", "tp"),
            P("tp", "kv"),
            P("kv", "tp", None, None),
        ),
        out_specs=(P(None, ("kv", "tp")), P("kv", "tp", None, None)),
        check_vma=False,
    )
```

time: 143 us -> 122 us (0.85)
  blocking collectives: 65.5 us -> 37.6 us
  waiting for transfers between devices: 27.5 us -> 32 us
  starting transfers between devices: 21.2 us -> 25 us
    all_to_all x6 -> x3, blocking collectives: 65.5 us -> 37.6 us  [the longest x2 23.8 us: gather_all(): lax.all_to_all(jnp.broadcast_to(value[None], (size, *value.shape)), axis,...]
    ppermute x0 -> x9, starting transfers between devices: none -> 13.3 us  [the longest x3 7.82 us: swap_cores(): return lax.ppermute(value, 'tp', [(i, i ^ 1) for i in range(8)])]
    ppermute x0 -> x9, waiting for transfers between devices: none -> 11.2 us  [the longest x6 8.53 us: shift_chips(): lax.ppermute(value, 'tp', [(i, (i + 2 * step) % 8) for i in range(8)])]
    all_to_all x4 -> x2, starting transfers between devices: 21.2 us -> 11.7 us  [the longest x1 7.77 us: spread_sum(): parts = lax.all_to_all(value, axis, 0, 0, tiled=True)]
    all_to_all x4 -> x2, waiting for transfers between devices: 27.5 us -> 20.9 us  [the longest x1 13.4 us: spread_sum(): parts = lax.all_to_all(value, axis, 0, 0, tiled=True)]
    unnamed x12 -> x11, local copies, waits for them, and re-layouts: 3.39 us -> 4.34 us
  transfers between devices with their start and end apart: 4 -> 11, of which waited for: 4 -> 9; matrix products, arithmetic and copies ran while one was open for 0% -> 0% of each run, Pallas kernels for 0% -> 0%
where the time goes in v1:
time: 122 us; the launch traced here: 121 us
  blocking collectives  37.6 us (31%)
  waiting for transfers between devices  32 us (26%)
  starting transfers between devices  25 us (20%)
  matrix products  12.5 us (10%)
  local copies, waits for them, and re-layouts  6.52 us (5%)
  other arithmetic  6.37 us (5%)
    all_to_all x2, blocking collectives, gather_all(): lax.all_to_all(jnp.broadcast_to(value[None], (size, *value.shape)), axis,...  23.8 us
    all_to_all x1, blocking collectives, spread_sum(): parts = lax.all_to_all(value, axis, 0, 0, tiled=True)  13.8 us
    all_to_all x1, waiting for transfers between devices, spread_sum(): parts = lax.all_to_all(value, axis, 0, 0, tiled=True)  13.4 us
    ppermute x6, waiting for transfers between devices, shift_chips(): lax.ppermute(value, 'tp', [(i, (i + 2 * step) % 8) for i in range(8)])  8.53 us
    ppermute x3, starting transfers between devices, swap_cores(): return lax.ppermute(value, 'tp', [(i, i ^ 1) for i in range(8)])  7.82 us
    all_to_all x1, starting transfers between devices, spread_sum(): parts = lax.all_to_all(value, axis, 0, 0, tiled=True)  7.77 us
    dot_general x4, matrix products, per_device(): jnp.dot(normed, w, preferred_element_type=F32).astype(BF16)  7.55 us
    all_to_all x1, waiting for transfers between devices, gather_all(): lax.all_to_all(jnp.broadcast_to(value[None], (size, *value.shape)), axis,...  7.53 us
  transfers between devices with their start and end apart: 11, of which 9 were waited for; matrix products, arithmetic and copies ran while one was open for 0% of the time, Pallas kernels for 0%

profile of v1, /device:TPU:1, one launch (start us, length us, event | category | flops | bytes accessed | tf_op | source)
XLA Modules:
  0.0 120.9 jit_solution(5850062174161661402)
XLA Ops:
  0.6 0.8 fusion.34
  1.5 10.5 %all_to_all.25 = bf16[8,40,128]{2,1,0:T(8,128)(2,1)S(1)} all-to-all(bf16[8,40,128]{2,1,0:T(8,128)(2,1)S(1)} %broadcast_in_dim.12), channel_id=1, replica_groups=mesh['kv'=16,'tp'=8] {'tp'}, dimensions={0} | all-to-all | bytes 163840 | tf_op jit(solution)/shard_map/all_to_all | solution.py:22
  12.0 0.1 copy.41
  12.2 0.1 multiply_reduce_fusion
  12.3 0.1 copy.42
  12.5 1.8 %fusion.3 = bf16[128,3200]{1,0:T(8,128)(2,1)} fusion(bf16[128,256]{1,0:T(8,128)(2,1)S(1)} %get-tuple-element.16, bf16[256,512]{1,0:T(8,128)(2,1)} %param.14), kind=kOutput, calls=%fused_computation.10 | convolution fusion | flops 33619968 | bytes 458752 | tf_op jit(solution)/shard_map/dot_general | solution.py:88
  14.3 1.8 %fusion.2 = bf16[128,3200]{1,0:T(8,128)(2,1)} fusion(bf16[128,3200]{1,0:T(8,128)(2,1)} %fusion.3, bf16[128,256]{1,0:T(8,128)(2,1)S(1)} %get-tuple-element.16, bf16[256,512]{1,0:T(8,128)(2,1)} %param.15), kind=kOutput, calls=%fused_computation.8 | convolution fusion | flops 33619968 | bytes 458752 | tf_op jit(solution)/shard_map/dot_general | solution.py:88
  16.1 2.0 %fusion.1 = bf16[128,3200]{1,0:T(8,128)(2,1)} fusion(bf16[128,3200]{1,0:T(8,128)(2,1)} %fusion.2, bf16[128,256]{1,0:T(8,128)(2,1)S(1)} %get-tuple-element.16, bf16[256,1024]{1,0:T(8,128)(2,1)} %param.16), kind=kOutput, calls=%fused_computation.6 | convolution fusion | flops 67239936 | bytes 851968 | tf_op jit(solution)/shard_map/dot_general | solution.py:88
  18.1 2.0 %fusion = bf16[128,3200]{1,0:T(8,128)(2,1)} fusion(bf16[128,3200]{1,0:T(8,128)(2,1)} %fusion.1, bf16[128,256]{1,0:T(8,128)(2,1)S(1)} %get-tuple-element.16, bf16[256,1024]{1,0:T(8,128)(2,1)} %param.17), kind=kOutput, calls=%fused_computation.4 | convolution fusion | flops 67239936 | bytes 851968 | tf_op jit(solution)/shard_map/dot_general | solution.py:88
  20.0 0.6 pad_dynamic-update-slice_fusion
  20.7 7.8 %all-to-all-start.1 = ((bf16[16,8,3200]{2,1,0:T(8,128)(2,1)}), bf16[16,8,3200]{2,1,0:T(8,128)(2,1)S(1)}, u32[]{:S(2)}, u32[]{:S(2)}) async-start(bf16[16,8,3200]{2,1,0:T(8,128)(2,1)} %bitcast.6), calls=%async_computation.1 | async-start | bytes 1638400 | tf_op jit(solution)/shard_map/all_to_all | solution.py:28
  28.5 13.4 %all-to-all-done.1 = bf16[16,8,3200]{2,1,0:T(8,128)(2,1)S(1)} async-done(((bf16[16,8,3200]{2,1,0:T(8,128)(2,1)}), bf16[16,8,3200]{2,1,0:T(8,128)(2,1)S(1)}, u32[]{:S(2)}, u32[]{:S(2)}) %all-to-all-start.1) | async-done | bytes 819232 | tf_op jit(solution)/shard_map/all_to_all | solution.py:28
  41.9 0.1 convert_reduce_fusion
  42.0 0.1 fusion.41
  42.3 4.1 %multiply_add_fusion = f32[8,2,256,512]{3,2,1,0:T(8,128)S(1)} fusion(f32[8,2,256,512]{3,2,1,0:T(8,128)} %param.21, f32[8,2,512]{2,1,0:T(2,128)S(1)} %copy.44, f32[8,2,256]{2,1,0:T(2,128)S(1)} %copy.43, f32[2]{0:T(128)S(1)} %dynamic_slice.19), kind=kLoop, calls=%fused_computation | loop fusion | flops 6291456 | bytes 16826376 | tf_op jit(solution)/shard_map/add | solution.py:46
  46.4 3.4 %copy-done.1 = f32[8,2,256,512]{3,2,1,0:T(8,128)} copy-done((f32[8,2,256,512]{3,2,1,0:T(8,128)}, f32[8,2,256,512]{3,2,1,0:T(8,128)S(1)}, u32[]{:S(2)}) %copy-start.1) | copy-done | bytes 8388632
  49.8 4.1 %fusion.31 = f32[8,2,1,512]{3,2,1,0:T(1,128)S(1)} fusion(f32[8,2,256,512]{3,2,1,0:T(8,128)S(1)} %multiply_add_fusion, f32[8,2,256,1]{2,0,1,3:T(8,128)S(1)} %bitcast.74), kind=kOutput, calls=%fused_computation.72 | convolution fusion | flops 25165824 | bytes 8437760 | tf_op jit(solution)/shard_map/shd,shde->she/dot_general | solution.py:47
  53.9 0.1 fusion.26
  54.0 0.1 multiply_convert_fusion.1
  54.1 0.7 broadcast_in_dim.13
  54.9 3.9 %all-to-all-start.2 = ((bf16[16,8,1024]{2,1,0:T(8,128)(2,1)}), bf16[16,8,1024]{2,1,0:T(8,128)(2,1)S(1)}, u32[]{:S(2)}, u32[]{:S(2)}) async-start(bf16[16,8,1024]{2,1,0:T(8,128)(2,1)} %broadcast_in_dim.13), calls=%async_computation.2 | async-start | bytes 524288 | tf_op jit(solution)/shard_map/all_to_all | solution.py:22
  58.8 7.5 %all-to-all-done.2 = bf16[16,8,1024]{2,1,0:T(8,128)(2,1)S(1)} async-done(((bf16[16,8,1024]{2,1,0:T(8,128)(2,1)}), bf16[16,8,1024]{2,1,0:T(8,128)(2,1)S(1)}, u32[]{:S(2)}, u32[]{:S(2)}) %all-to-all-start.2) | async-done | bytes 262176 | tf_op jit(solution)/shard_map/all_to_all | solution.py:22
  66.3 0.2 convolution_convert_fusion.6
  66.6 3.2 %collective-permute-start = (bf16[128,128]{1,0:T(8,128)(2,1)S(1)}, bf16[128,128]{1,0:T(8,128)(2,1)S(1)}, u32[]{:S(2)}, u32[]{:S(2)}) collective-permute-start(bf16[128,128]{1,0:T(8,128)(2,1)S(1)} %broadcast_select_fusion.2), channel_id=1, source_target_pairs={{0,1},{1,0},{2,3},{3,2},{4,5},{5,4},{6,7},{7,6},{8,9},{9,8},{10,11... | collective-permute-start | bytes 98312 | tf_op jit(solution)/shard_map/ppermute | solution.py:33
  69.8 0.9 collective-permute-done
  70.7 0.4 collective-permute-start.1
  71.0 2.4 %collective-permute-start.2 = (bf16[128,128]{1,0:T(8,128)(2,1)S(1)}, bf16[128,128]{1,0:T(8,128)(2,1)S(1)}, u32[]{:S(2)}, u32[]{:S(2)}) collective-permute-start(bf16[128,128]{1,0:T(8,128)(2,1)S(1)} %add_convert_fusion), channel_id=1, source_target_pairs={{0,6},{1,7},{2,0},{3,1},{4,2},{5,3},{6,4},{7,5},{8,14},{9,15},{10,... | collective-permute-start | bytes 98312 | tf_op jit(solution)/shard_map/ppermute | solution.py:37
  73.4 1.3 %collective-permute-done.1 = bf16[128,128]{1,0:T(8,128)(2,1)S(1)} collective-permute-done((bf16[128,128]{1,0:T(8,128)(2,1)S(1)}, bf16[128,128]{1,0:T(8,128)(2,1)S(1)}, u32[]{:S(2)}, u32[]{:S(2)}) %collective-permute-start.1) | collective-permute-done | bytes 32800 | tf_op jit(solution)/shard_map/ppermute | solution.py:37
  74.7 3.0 %collective-permute-done.3 = bf16[128,128]{1,0:T(8,128)(2,1)S(1)} collective-permute-done((bf16[128,128]{1,0:T(8,128)(2,1)S(1)}, bf16[128,128]{1,0:T(8,128)(2,1)S(1)}, u32[]{:S(2)}, u32[]{:S(2)}) %collective-permute-start.3) | collective-permute-done | bytes 32800 | tf_op jit(solution)/shard_map/ppermute | solution.py:37
  77.7 2.1 %collective-permute-start.4 = (bf16[128,128]{1,0:T(8,128)(2,1)S(1)}, bf16[128,128]{1,0:T(8,128)(2,1)S(1)}, u32[]{:S(2)}, u32[]{:S(2)}) collective-permute-start(bf16[128,128]{1,0:T(8,128)(2,1)S(1)} %fusion.18), channel_id=1, source_target_pairs={{0,1},{1,0},{2,3},{3,2},{4,5},{5,4},{6,7},{7,6},{8,9},{9,8},{10,11... | collective-permute-start | bytes 98312 | tf_op jit(solution)/shard_map/ppermute | solution.py:33
  79.9 0.8 collective-permute-done.4
  80.7 0.1 fusion.12
  80.8 0.1 copy.45
  81.0 0.3 convolution_convert_fusion
  81.4 13.8 %all_to_all.26 = bf16[16,8,2176]{2,1,0:T(8,128)(2,1)S(1)} all-to-all(bf16[16,8,2176]{2,1,0:T(8,128)(2,1)S(1)} %fusion.7), channel_id=1, replica_groups=mesh['kv'=16,'tp'=8] {'kv'}, dimensions={0} | all-to-all | bytes 1114112 | tf_op jit(solution)/shard_map/all_to_all | solution.py:28
  95.2 0.1 fusion.37
  95.5 13.3 %all_to_all.27 = bf16[16,8,2048]{2,1,0:T(8,128)(2,1)S(1)} all-to-all(bf16[16,8,2048]{2,1,0:T(8,128)(2,1)S(1)} %broadcast_in_dim.14), channel_id=1, replica_groups=mesh['kv'=16,'tp'=8] {'kv'}, dimensions={0} | all-to-all | bytes 1048576 | tf_op jit(solution)/shard_map/all_to_all | solution.py:22
  108.8 0.3 fusion.4
  109.1 0.1 copy.46
  109.3 0.1 copy.52
  109.4 0.1 copy.53
  109.6 2.5 %collective-permute-start.5 = (bf16[4,32,128]{1,2,0:T(8,128)(2,1)S(1)}, bf16[4,32,128]{1,2,0:T(8,128)(2,1)S(1)}, u32[]{:S(2)}, u32[]{:S(2)}) collective-permute-start(bf16[4,32,128]{1,2,0:T(8,128)(2,1)S(1)} %select_bitcast_fusion), channel_id=1, source_target_pairs={{0,1},{1,0},{2,3},{3,2},{4,5},{5,4},{6,7},{7,6},{8,9},{9,8},{10,11... | collective-permute-start | bytes 98312 | tf_op jit(solution)/shard_map/ppermute | solution.py:33
  112.0 1.0 collective-permute-done.5
  113.2 2.7 %collective-permute-start.7 = (bf16[32,128]{0,1:T(8,128)(2,1)S(1)}, bf16[32,128]{0,1:T(8,128)(2,1)S(1)}, u32[]{:S(2)}, u32[]{:S(2)}) collective-permute-start(bf16[32,128]{0,1:T(8,128)(2,1)S(1)} %get-tuple-element.14), channel_id=1, source_target_pairs={{0,6},{1,7},{2,0},{3,1},{4,2},{5,3},{6,4},{7,5},{8,14},{9,15},{10,... | collective-permute-start | bytes 24584 | tf_op jit(solution)/shard_map/ppermute | solution.py:37
  115.8 1.3 %collective-permute-done.6 = bf16[32,128]{0,1:T(8,128)(2,1)S(1)} collective-permute-done((bf16[32,128]{0,1:T(8,128)(2,1)S(1)}, bf16[32,128]{0,1:T(8,128)(2,1)S(1)}, u32[]{:S(2)}, u32[]{:S(2)}) %collective-permute-start.6) | collective-permute-done | bytes 8224 | tf_op jit(solution)/shard_map/ppermute | solution.py:37
  117.1 3.0 %collective-permute-done.8 = bf16[32,128]{0,1:T(8,128)(2,1)S(1)} collective-permute-done((bf16[32,128]{0,1:T(8,128)(2,1)S(1)}, bf16[32,128]{0,1:T(8,128)(2,1)S(1)}, u32[]{:S(2)}, u32[]{:S(2)}) %collective-permute-start.8) | collective-permute-done | bytes 8224 | tf_op jit(solution)/shard_map/ppermute | solution.py:37
  120.1 0.1 fusion.24
  120.2 0.7 copy.49
  (38 shorter events, 1.1 us)
Async XLA Ops:
  0.6 80.4 %copy-start = (bf16[256,2048]{1,0:T(8,128)(2,1)S(1)}, bf16[256,2048]{1,0:T(8,128)(2,1)}, u32[]{:S(2)}) copy-start(bf16[256,2048]{1,0:T(8,128)(2,1)} %param.19) | copy-start | bytes 3145732
  20.7 21.2 %all-to-all-start.1 = ((bf16[16,8,3200]{2,1,0:T(8,128)(2,1)}), bf16[16,8,3200]{2,1,0:T(8,128)(2,1)S(1)}, u32[]{:S(2)}, u32[]{:S(2)}) async-start(bf16[16,8,3200]{2,1,0:T(8,128)(2,1)} %bitcast.6), calls=%async_computation.1 | async-start | bytes 1638400 | tf_op jit(solution)/shard_map/all_to_all | solution.py:28
  46.4 3.4 %copy-start.1 = (f32[8,2,256,512]{3,2,1,0:T(8,128)}, f32[8,2,256,512]{3,2,1,0:T(8,128)S(1)}, u32[]{:S(2)}) copy-start(f32[8,2,256,512]{3,2,1,0:T(8,128)S(1)} %multiply_add_fusion) | copy-start | bytes 25165828
  46.4 19.9 %copy-start.3 = (bf16[1024,256]{1,0:T(8,128)(2,1)S(1)}, bf16[1024,256]{1,0:T(8,128)(2,1)}, u32[]{:S(2)}) copy-start(bf16[1024,256]{1,0:T(8,128)(2,1)} %param.18) | copy-start | bytes 1572868
  49.8 59.0 %copy-start.2 = (bf16[2048,256]{1,0:T(8,128)(2,1)S(1)}, bf16[2048,256]{1,0:T(8,128)(2,1)}, u32[]{:S(2)}) copy-start(bf16[2048,256]{1,0:T(8,128)(2,1)} %param.20) | copy-start | bytes 3145732
  54.9 11.5 %all-to-all-start.2 = ((bf16[16,8,1024]{2,1,0:T(8,128)(2,1)}), bf16[16,8,1024]{2,1,0:T(8,128)(2,1)S(1)}, u32[]{:S(2)}, u32[]{:S(2)}) async-start(bf16[16,8,1024]{2,1,0:T(8,128)(2,1)} %broadcast_in_dim.13), calls=%async_computation.2 | async-start | bytes 524288 | tf_op jit(solution)/shard_map/all_to_all | solution.py:22
  66.6 4.1 %collective-permute-start = (bf16[128,128]{1,0:T(8,128)(2,1)S(1)}, bf16[128,128]{1,0:T(8,128)(2,1)S(1)}, u32[]{:S(2)}, u32[]{:S(2)}) collective-permute-start(bf16[128,128]{1,0:T(8,128)(2,1)S(1)} %broadcast_select_fusion.2), channel_id=1, source_target_pairs={{0,1},{1,0},{2,3},{3,2},{4,5},{5,4},{6,7},{7,6},{8,9},{9,8},{10,11... | collective-permute-start | bytes 98312 | tf_op jit(solution)/shard_map/ppermute | solution.py:33
  70.7 4.0 %collective-permute-start.1 = (bf16[128,128]{1,0:T(8,128)(2,1)S(1)}, bf16[128,128]{1,0:T(8,128)(2,1)S(1)}, u32[]{:S(2)}, u32[]{:S(2)}) collective-permute-start(bf16[128,128]{1,0:T(8,128)(2,1)S(1)} %add_convert_fusion), channel_id=1, source_target_pairs={{0,2},{1,3},{2,4},{3,5},{4,6},{5,7},{6,0},{7,1},{8,10},{9,11},{10,... | collective-permute-start | bytes 98312 | tf_op jit(solution)/shard_map/ppermute | solution.py:37
  71.0 3.7 %collective-permute-start.2 = (bf16[128,128]{1,0:T(8,128)(2,1)S(1)}, bf16[128,128]{1,0:T(8,128)(2,1)S(1)}, u32[]{:S(2)}, u32[]{:S(2)}) collective-permute-start(bf16[128,128]{1,0:T(8,128)(2,1)S(1)} %add_convert_fusion), channel_id=1, source_target_pairs={{0,6},{1,7},{2,0},{3,1},{4,2},{5,3},{6,4},{7,5},{8,14},{9,15},{10,... | collective-permute-start | bytes 98312 | tf_op jit(solution)/shard_map/ppermute | solution.py:37
  73.4 4.3 %collective-permute-start.3 = (bf16[128,128]{1,0:T(8,128)(2,1)S(1)}, bf16[128,128]{1,0:T(8,128)(2,1)S(1)}, u32[]{:S(2)}, u32[]{:S(2)}) collective-permute-start(bf16[128,128]{1,0:T(8,128)(2,1)S(1)} %add_convert_fusion), channel_id=1, source_target_pairs={{0,4},{1,5},{2,6},{3,7},{4,0},{5,1},{6,2},{7,3},{8,12},{9,13},{10,... | collective-permute-start | bytes 98312 | tf_op jit(solution)/shard_map/ppermute | solution.py:37
  77.7 3.0 %collective-permute-start.4 = (bf16[128,128]{1,0:T(8,128)(2,1)S(1)}, bf16[128,128]{1,0:T(8,128)(2,1)S(1)}, u32[]{:S(2)}, u32[]{:S(2)}) collective-permute-start(bf16[128,128]{1,0:T(8,128)(2,1)S(1)} %fusion.18), channel_id=1, source_target_pairs={{0,1},{1,0},{2,3},{3,2},{4,5},{5,4},{6,7},{7,6},{8,9},{9,8},{10,11... | collective-permute-start | bytes 98312 | tf_op jit(solution)/shard_map/ppermute | solution.py:33
  109.6 3.4 %collective-permute-start.5 = (bf16[4,32,128]{1,2,0:T(8,128)(2,1)S(1)}, bf16[4,32,128]{1,2,0:T(8,128)(2,1)S(1)}, u32[]{:S(2)}, u32[]{:S(2)}) collective-permute-start(bf16[4,32,128]{1,2,0:T(8,128)(2,1)S(1)} %select_bitcast_fusion), channel_id=1, source_target_pairs={{0,1},{1,0},{2,3},{3,2},{4,5},{5,4},{6,7},{7,6},{8,9},{9,8},{10,11... | collective-permute-start | bytes 98312 | tf_op jit(solution)/shard_map/ppermute | solution.py:33
  113.1 4.0 %collective-permute-start.6 = (bf16[32,128]{0,1:T(8,128)(2,1)S(1)}, bf16[32,128]{0,1:T(8,128)(2,1)S(1)}, u32[]{:S(2)}, u32[]{:S(2)}) collective-permute-start(bf16[32,128]{0,1:T(8,128)(2,1)S(1)} %get-tuple-element.12), channel_id=1, source_target_pairs={{0,2},{1,3},{2,4},{3,5},{4,6},{5,7},{6,0},{7,1},{8,10},{9,11},{10,... | collective-permute-start | bytes 24584 | tf_op jit(solution)/shard_map/ppermute | solution.py:37
  113.2 4.0 %collective-permute-start.7 = (bf16[32,128]{0,1:T(8,128)(2,1)S(1)}, bf16[32,128]{0,1:T(8,128)(2,1)S(1)}, u32[]{:S(2)}, u32[]{:S(2)}) collective-permute-start(bf16[32,128]{0,1:T(8,128)(2,1)S(1)} %get-tuple-element.14), channel_id=1, source_target_pairs={{0,6},{1,7},{2,0},{3,1},{4,2},{5,3},{6,4},{7,5},{8,14},{9,15},{10,... | collective-permute-start | bytes 24584 | tf_op jit(solution)/shard_map/ppermute | solution.py:37
  115.8 4.3 %collective-permute-start.8 = (bf16[32,128]{0,1:T(8,128)(2,1)S(1)}, bf16[32,128]{0,1:T(8,128)(2,1)S(1)}, u32[]{:S(2)}, u32[]{:S(2)}) collective-permute-start(bf16[32,128]{0,1:T(8,128)(2,1)S(1)} %get-tuple-element.13), channel_id=1, source_target_pairs={{0,4},{1,5},{2,6},{3,7},{4,0},{5,1},{6,2},{7,3},{8,12},{9,13},{10,... | collective-permute-start | bytes 24584 | tf_op jit(solution)/shard_map/ppermute | solution.py:37

commit v2 on v1

v2 whole, which is shorter than its diff:
```python
import jax
import jax.numpy as jnp
from jax import lax
from jax.experimental import pallas as pl
from jax.experimental.pallas import tpu as pltpu
from jax.sharding import PartitionSpec as P

D = 4096
HEADS = 16
DK = 256
DV = 512
EPS = 1e-06
F32 = jnp.float32
BF16 = jnp.bfloat16
VMEM = pl.BlockSpec(memory_space=pltpu.VMEM)
SMEM = pl.BlockSpec(memory_space=pltpu.SMEM)
HBM = pl.BlockSpec(memory_space=pltpu.HBM)


def in_hbm(value):
    return pltpu.with_memory_space_constraint(value, pltpu.HBM)


def gather_all(value, axis):
    size = lax.axis_size(axis)
    return lax.all_to_all(
        jnp.broadcast_to(value[None], (size, *value.shape)), axis, 0, 0, tiled=True
    )


def swap_cores(value):
    return lax.ppermute(value, "tp", [(i, i ^ 1) for i in range(8)])


def swap_chips(value, mask):
    return lax.ppermute(value, "tp", [(i, i ^ (2 * mask)) for i in range(8)])


def squares_lanes(total, width):
    lane = lax.broadcasted_iota(jnp.int32, (total.shape[0], width), 1)
    high = total.astype(BF16).astype(F32)
    return jnp.where(lane == 0, high, jnp.where(lane == 1, total - high, 0.0)).astype(BF16)


def project_body(packed, wq, wk, wv, wg, terms, stream_out, gains_out, bq, bk, bv, bg, sems):
    pairs = ((wq, bq), (wk, bk), (wv, bv), (wg, bg))
    copies = [pltpu.make_async_copy(w, buf, sems.at[i]) for i, (w, buf) in enumerate(pairs)]
    for copy in copies:
        copy.start()
    stream = packed[:, :32, :].astype(F32).reshape(256, 128).T
    stream_out[...] = stream.astype(BF16)
    gains = jnp.sum(packed[:, 32:40, :].astype(F32), axis=0)
    gains_out[...] = gains
    mixer = jnp.concatenate([gains[0:1], gains[1:2]], axis=1)
    normed = (stream * mixer).astype(BF16)
    terms[:, 3072:] = squares_lanes(jnp.sum(stream * stream, axis=1, keepdims=True), 128)
    at = 0
    for copy, (_, buf) in zip(copies, pairs):
        n = buf.shape[1]
        copy.wait()
        terms[:, at : at + n] = jnp.dot(normed, buf[...], preferred_element_type=F32).astype(BF16)
        at += n


def retain_body(rates, parts, state_hbm, mixed_out, key_out, value_out, kept, state, sems):
    copies = [pltpu.make_async_copy(state_hbm.at[b], state.at[b], sems.at[b]) for b in range(8)]
    for copy in copies:
        copy.start()
    sums = jnp.sum(parts[...].astype(F32), axis=0)
    scale = lax.rsqrt((sums[:, 3072:3073] + sums[:, 3073:3074]) / D + EPS)
    query = scale * sums[:, :512]
    key = scale * sums[:, 512:1024] * DK ** (-0.5)
    value = scale * sums[:, 1024:2048]
    gate = scale * sums[:, 2048:3072]
    query_t = query.T
    key_out[...] = key.T
    value_out[...] = value
    for b in range(8):
        copies[b].wait()
        for h in range(2):
            total = jnp.zeros((8, 512), F32)
            for r in range(0, 256, 64):
                qc = query_t[h * 256 + r : h * 256 + r + 64, b : b + 1]
                total = total + jnp.sum((qc * state[b, h, r : r + 64, :]).reshape(8, 8, 512), axis=0)
            kept[b : b + 1, h * 512 : (h + 1) * 512] = jnp.sum(total, axis=0, keepdims=True)
    for h in range(2):
        cols = slice(h * 512, (h + 1) * 512)
        heads = slice(h * 256, (h + 1) * 256)
        match = jnp.sum(query[:, heads] * key[:, heads], axis=1, keepdims=True)
        out = rates[h] * kept[:, cols] + match * value[:, cols]
        out = out * lax.rsqrt(jnp.mean(out * out, axis=1, keepdims=True) + EPS)
        g = gate[:, cols]
        mixed = (g * jax.nn.sigmoid(g) * out).astype(BF16)
        for j in range(16):
            mixed_out[j, :, cols] = mixed


def advance_body(rates, key_t, value, state_hbm, new_hbm, state, new, in_sems, out_sems):
    reads = [pltpu.make_async_copy(state_hbm.at[b], state.at[b], in_sems.at[b]) for b in range(8)]
    writes = [pltpu.make_async_copy(new.at[b], new_hbm.at[b], out_sems.at[b]) for b in range(8)]
    for copy in reads:
        copy.start()
    for b in range(8):
        reads[b].wait()
        for h in range(2):
            row = value[b : b + 1, h * 512 : (h + 1) * 512]
            for r in range(0, 256, 64):
                kc = key_t[h * 256 + r : h * 256 + r + 64, b : b + 1]
                new[b, h, r : r + 64, :] = rates[h] * state[b, h, r : r + 64, :] + kc * row
        writes[b].start()
    for copy in writes:
        copy.wait()


def per_device(
    activations,
    mixer_gain,
    channel_gain,
    query_weight,
    key_weight,
    value_weight,
    gate_weight,
    output_weight,
    up_weight,
    down_weight,
    state_in,
):
    tp = lax.axis_index("tp")
    core = tp % 2
    chip = tp // 2
    heads_dev = state_in.shape[1]
    index = (tp * heads_dev + jnp.arange(heads_dev, dtype=jnp.int32)).astype(F32)
    rates = 1.0 - 2.0 ** (-1.0 - 6.0 * index / (HEADS - 1))

    spread = jnp.arange(128) // 32 == tp % 4
    tiled = [jnp.where(spread, jnp.tile(g, 4), 0) for g in (mixer_gain, channel_gain)]
    row = jnp.arange(8)[:, None]
    first = tp // 4
    gain_rows = jnp.where(row == first, tiled[0], jnp.where(row == first + 2, tiled[1], 0))
    rows = jnp.concatenate([activations.T, gain_rows.astype(BF16)], axis=0)
    rows, rates = lax.optimization_barrier((rows, rates))
    packed = gather_all(rows, "tp")

    weights = (query_weight, key_weight, value_weight, gate_weight)
    terms, stream, gains = pl.pallas_call(
        project_body,
        out_shape=(
            jax.ShapeDtypeStruct((128, 3200), BF16),
            jax.ShapeDtypeStruct((128, 256), BF16),
            jax.ShapeDtypeStruct((8, 128), F32),
        ),
        in_specs=[VMEM, HBM, HBM, HBM, HBM],
        out_specs=(VMEM, VMEM, VMEM),
        scratch_shapes=[pltpu.VMEM(w.shape, BF16) for w in weights]
        + [pltpu.SemaphoreType.DMA((4,))],
        compiler_params=pltpu.CompilerParams(vmem_limit_bytes=16 << 20),
        name="project",
    )(packed, *map(in_hbm, weights))
    channel = jnp.concatenate([gains[2:3], gains[3:4]], axis=1)
    stream = stream.astype(F32)
    parts = lax.all_to_all(terms.reshape(16, 8, 3200), "kv", 0, 0, tiled=True)

    state = in_hbm(state_in)
    mixed, key_t, value = pl.pallas_call(
        retain_body,
        out_shape=(
            jax.ShapeDtypeStruct((16, 8, 1024), BF16),
            jax.ShapeDtypeStruct((512, 8), F32),
            jax.ShapeDtypeStruct((8, 1024), F32),
        ),
        in_specs=[SMEM, VMEM, HBM],
        out_specs=(VMEM, VMEM, VMEM),
        scratch_shapes=[
            pltpu.VMEM((8, 1024), F32),
            pltpu.VMEM(state_in.shape, F32),
            pltpu.SemaphoreType.DMA((8,)),
        ],
        compiler_params=pltpu.CompilerParams(vmem_limit_bytes=16 << 20),
        name="retain",
    )(rates, parts, state)
    new_state = pl.pallas_call(
        advance_body,
        out_shape=jax.ShapeDtypeStruct(state_in.shape, F32),
        in_specs=[SMEM, VMEM, VMEM, HBM],
        out_specs=HBM,
        scratch_shapes=[
            pltpu.VMEM(state_in.shape, F32),
            pltpu.VMEM(state_in.shape, F32),
            pltpu.SemaphoreType.DMA((8,)),
            pltpu.SemaphoreType.DMA((8,)),
        ],
        compiler_params=pltpu.CompilerParams(vmem_limit_bytes=24 << 20),
        cost_estimate=pl.CostEstimate(flops=40_000_000, transcendentals=0, bytes_accessed=16 << 20),
        name="advance",
    )(rates, key_t, value, state)

    mixed_all = lax.all_to_all(mixed, "kv", 0, 0, tiled=True)
    mixed_all, new_state = lax.optimization_barrier((mixed_all, new_state))
    mixed_all = mixed_all.reshape(128, 1024)
    out_terms = jnp.dot(mixed_all, output_weight, preferred_element_type=F32).astype(BF16)
    halves = (out_terms[:, :128], out_terms[:, 128:])
    mine = jnp.where(core == 0, halves[0], halves[1])
    theirs = jnp.where(core == 0, halves[1], halves[0])
    pair = (mine.astype(F32) + swap_cores(theirs).astype(F32)).astype(BF16)
    quad = (pair.astype(F32) + swap_chips(pair, 1).astype(F32)).astype(BF16)
    attention = quad.astype(F32) + swap_chips(quad, 3).astype(F32)
    stream_half = jnp.where(core == 0, stream[:, :128], stream[:, 128:])
    middle_half = (stream_half + attention).astype(BF16)
    other_half = swap_cores(middle_half)
    middle_bf = jnp.concatenate(
        [
            jnp.where(core == 0, middle_half, other_half),
            jnp.where(core == 0, other_half, middle_half),
        ],
        axis=1,
    )
    middle = middle_bf.astype(F32)
    middle_squares = jnp.sum(middle * middle, axis=1, keepdims=True)
    channel_normed = (middle * channel).astype(BF16)
    up_terms = jnp.concatenate(
        [
            jnp.dot(channel_normed, up_weight, preferred_element_type=F32).astype(BF16),
            jnp.pad(middle_squares.astype(BF16), ((0, 0), (0, 127))),
        ],
        axis=1,
    )
    up_parts = lax.all_to_all(up_terms.reshape(16, 8, -1), "kv", 0, 0, tiled=True)
    up_sum = jnp.sum(up_parts.astype(F32), axis=0)
    lifted = lax.rsqrt(up_sum[:, 2048:2049] / D + EPS) * up_sum[:, :2048]
    hidden = jnp.square(jax.nn.relu(lifted)).astype(BF16)

    hidden_all = gather_all(hidden, "kv").reshape(128, 2048)
    down_terms = jnp.dot(hidden_all, down_weight, preferred_element_type=F32).astype(BF16)
    down_t = down_terms.T.reshape(4, 2, 32, 128)
    mine = jnp.where(core == 0, down_t[:, 0], down_t[:, 1])
    theirs = jnp.where(core == 0, down_t[:, 1], down_t[:, 0])
    pair = (mine.astype(F32) + swap_cores(theirs).astype(F32)).astype(BF16)
    keep = jnp.stack([lax.dynamic_index_in_dim(pair, chip ^ m, 0, keepdims=False) for m in (0, 3)])
    give = jnp.stack([lax.dynamic_index_in_dim(pair, chip ^ m, 0, keepdims=False) for m in (1, 2)])
    keep = keep.astype(F32) + swap_chips(give, 1).astype(F32)
    lowered = keep[0] + swap_chips(keep[1].astype(BF16), 3).astype(F32)
    own = lax.dynamic_slice_in_dim(middle_bf.T, tp * 32, 32, 0).astype(F32)
    return ((own + lowered).astype(BF16).T, new_state)


def solution(mesh):
    return jax.shard_map(
        per_device,
        mesh=mesh,
        in_specs=(
            P(None, ("kv", "tp")),
            P(("kv", "tp")),
            P(("kv", "tp")),
            P("kv", "tp"),
            P("kv", "tp"),
            P("kv", "tp"),
            P("kv", "tp"),
            P("tp", "kv"),
            P("kv", "tp"),
            P("tp", "kv"),
            P("kv", "tp", None, None),
        ),
        out_specs=(P(None, ("kv", "tp")), P("kv", "tp", None, None)),
        check_vma=False,
    )
```

time: 122 us -> 113 us (0.926)
  blocking collectives: 37.6 us -> 61.8 us
  waiting for transfers between devices: 32 us -> 14.2 us
  Pallas kernels: 0 us -> 14.5 us
  matrix products: 12.5 us -> 0.85 us
  starting transfers between devices: 25 us -> 14.2 us
  other arithmetic: 6.37 us -> 1.46 us
  local copies, waits for them, and re-layouts: 6.52 us -> 2.82 us
    all_to_all x1 -> x2, blocking collectives: 13.8 us -> 38 us  [the longest x1 21.3 us: per_device(): parts = lax.all_to_all(terms.reshape(16, 8, 3200), 'kv', 0, 0, tiled=True)]
    all_to_all x2 -> x1, waiting for transfers between devices: 20.9 us -> 0.03 us  [per_device(): mixed_all = lax.all_to_all(mixed, 'kv', 0, 0, tiled=True)]
    pallas_call x0 -> x3, Pallas kernels: none -> 14.5 us  [the longest x1 7.47 us: per_device(): pl.pallas_call(advance_body, out_shape=jax.ShapeDtypeStruct(state_in.shap...]
    dot_general x5 -> x0, matrix products: 11.6 us -> none  [the longest x4 7.55 us: per_device(): jnp.dot(normed, w, preferred_element_type=F32).astype(BF16)]
    all_to_all x2 -> x1, starting transfers between devices: 11.7 us -> 3.54 us  [per_device(): mixed_all = lax.all_to_all(mixed, 'kv', 0, 0, tiled=True)]
    add x1, other arithmetic: 4.05 us -> 0.01 us  [per_device(): keep = keep.astype(F32) + swap_chips(give, 1).astype(F32)]
    unnamed x11 -> x7, local copies, waits for them, and re-layouts: 4.34 us -> 0.7 us
    ppermute x6 -> x4, starting transfers between devices: 5.49 us -> 2.38 us  [swap_chips(): return lax.ppermute(value, 'tp', [(i, i ^ 2 * mask) for i in range(8)])]
  transfers between devices with their start and end apart: 11 -> 8, of which waited for: 9 -> 7; matrix products, arithmetic and copies ran while one was open for 0% -> 0% of each run, Pallas kernels for 0% -> 7%
where the time goes in v2:
time: 113 us; the launch traced here: 111 us
  blocking collectives  61.8 us (55%)
  Pallas kernels  14.5 us (13%)
  starting transfers between devices  14.2 us (13%)
  waiting for transfers between devices  14.2 us (13%)
  local copies, waits for them, and re-layouts  2.82 us (2%)
  other arithmetic  1.46 us (1%)
    all_to_all x2, blocking collectives, gather_all(): lax.all_to_all(jnp.broadcast_to(value[None], (size, *value.shape)), axis,...  23.8 us
    all_to_all x1, blocking collectives, per_device(): parts = lax.all_to_all(terms.reshape(16, 8, 3200), 'kv', 0, 0, tiled=True)  21.3 us
    all_to_all x1, blocking collectives, per_device(): lax.all_to_all(up_terms.reshape(16, 8, -1), 'kv', 0, 0, tiled=True)  16.7 us
    ppermute x4, waiting for transfers between devices, swap_chips(): return lax.ppermute(value, 'tp', [(i, i ^ 2 * mask) for i in range(8)])  11.6 us
    ppermute x3, starting transfers between devices, swap_cores(): return lax.ppermute(value, 'tp', [(i, i ^ 1) for i in range(8)])  8.28 us
    pallas_call x1, Pallas kernels, per_device(): pl.pallas_call(advance_body, out_shape=jax.ShapeDtypeStruct(state_in.shap...  7.47 us
    pallas_call x1, Pallas kernels, per_device(): pl.pallas_call(retain_body, out_shape=(jax.ShapeDtypeStruct((16, 8, 1024)...  5.19 us
    all_to_all x1, starting transfers between devices, per_device(): mixed_all = lax.all_to_all(mixed, 'kv', 0, 0, tiled=True)  3.54 us
  transfers between devices with their start and end apart: 8, of which 7 were waited for; matrix products, arithmetic and copies ran while one was open for 0% of the time, Pallas kernels for 7%

profile of v2, /device:TPU:1, one launch (start us, length us, event | category | flops | bytes accessed | tf_op | source)
XLA Modules:
  0.0 110.8 jit_solution(8816384939677718520)
XLA Ops:
  0.6 0.0 copy-start
  0.7 0.7 tile.8
  1.4 0.1 tile.9
  1.5 0.7 tile.20
  2.2 0.1 tile.21
  2.3 0.1 select_select_fusion
  2.4 0.7 pad_maximum_fusion.3
  3.1 10.5 %all_to_all.25.packed = bf16[8,40,128]{2,1,0:T(8,128)(2,1)S(1)} all-to-all(bf16[8,40,128]{2,1,0:T(8,128)(2,1)S(1)} %broadcast_in_dim.53), channel_id=1, replica_groups=mesh['kv'=16,'tp'=8] {'tp'}, dimensions={0} | all-to-all | bytes 163840 | tf_op jit(solution)/shard_map/all_to_all | solution.py:26
  13.6 1.8 %project.1 = (bf16[128,3200]{1,0:T(8,128)(2,1)S(1)}, bf16[128,256]{1,0:T(8,128)(2,1)S(1)}, f32[8,128]{1,0:T(8,128)S(1)}) custom-call(bf16[8,40,128]{2,1,0:T(8,128)(2,1)S(1)} %all_to_all.25.packed, bf16[256,512]{1,0:T(8,128)(2,1)} %wq.1, bf16[256,512]{1,0:T(8,128)(2,1)} %wk.1, bf16[256,1024]{1,0:T(8,128)(2,1)} %wv.1, bf16[256,1024]{1,0:T(8,128)(2,1)} %wg.1), custom_call_target="tpu_custom_call" | custom-call | tf_op jit(solution)/shard_map/project/pallas_call | solution.py:145
  15.4 21.3 %all_to_all.26.parts = bf16[16,8,3200]{2,1,0:T(8,128)(2,1)S(1)} all-to-all(bf16[16,8,3200]{2,1,0:T(8,128)(2,1)S(1)} %bitcast.59), channel_id=1, replica_groups=mesh['kv'=16,'tp'=8] {'kv'}, dimensions={0} | all-to-all | bytes 1638400 | tf_op jit(solution)/shard_map/all_to_all | solution.py:161
  36.7 5.2 %retain.1 = (bf16[16,8,1024]{2,1,0:T(8,128)(2,1)}, f32[512,8]{1,0:T(8,128)S(1)}, f32[8,1024]{1,0:T(8,128)S(1)}) custom-call(f32[2]{0:T(128)S(1)} %power_subtract_fusion.rates, bf16[16,8,3200]{2,1,0:T(8,128)(2,1)S(1)} %all_to_all.26.parts, f32[8,2,256,512]{3,2,1,0:T(8,128)} %state_hbm.3), custom_call_target="tpu_custom_call" | custom-call | tf_op jit(solution)/shard_map/retain/pallas_call | solution.py:164
  41.9 3.5 %all-to-all-start.2 = ((bf16[16,8,1024]{2,1,0:T(8,128)(2,1)}), bf16[16,8,1024]{2,1,0:T(8,128)(2,1)S(1)}, u32[]{:S(2)}, u32[]{:S(2)}) async-start(bf16[16,8,1024]{2,1,0:T(8,128)(2,1)} %get-tuple-element.16), calls=%async_computation.2 | async-start | bytes 524288 | tf_op jit(solution)/shard_map/all_to_all | solution.py:197
  45.5 0.0 copy-start.2
  45.5 7.5 %advance.1 = f32[8,2,256,512]{3,2,1,0:T(8,128)} custom-call(f32[2]{0:T(128)S(1)} %power_subtract_fusion.rates, f32[512,8]{1,0:T(8,128)S(1)} %get-tuple-element.17.key_t, f32[8,1024]{1,0:T(8,128)S(1)} %get-tuple-element.18.value, f32[8,2,256,512]{3,2,1,0:T(8,128)} %state_hbm.3), custom_call_target="tpu_custom_call" | custom-call | flops 40000000 | bytes 16777216 | tf_op jit(solution)/shard_map/advance/pallas_call | solution.py:181
  53.0 0.0 all-to-all-done.2
  53.0 0.0 copy-done.2
  53.0 0.2 convolution_convert_fusion.2
  53.3 3.1 %collective-permute-start = (bf16[128,128]{1,0:T(8,128)(2,1)S(1)}, bf16[128,128]{1,0:T(8,128)(2,1)S(1)}, u32[]{:S(2)}, u32[]{:S(2)}) collective-permute-start(bf16[128,128]{1,0:T(8,128)(2,1)S(1)} %broadcast_select_fusion.2), channel_id=1, source_target_pairs={{0,1},{1,0},{2,3},{3,2},{4,5},{5,4},{6,7},{7,6},{8,9},{9,8},{10,11... | collective-permute-start | bytes 98312 | tf_op jit(solution)/shard_map/ppermute | solution.py:32
  56.4 0.9 collective-permute-done
  57.3 0.4 collective-permute-start.1
  57.6 2.5 %collective-permute-done.1 = bf16[128,128]{1,0:T(8,128)(2,1)S(1)} collective-permute-done((bf16[128,128]{1,0:T(8,128)(2,1)S(1)}, bf16[128,128]{1,0:T(8,128)(2,1)S(1)}, u32[]{:S(2)}, u32[]{:S(2)}) %collective-permute-start.1) | collective-permute-done | bytes 32800 | tf_op jit(solution)/shard_map/ppermute | solution.py:36
  60.1 1.0 collective-permute-start.2
  61.1 3.1 %collective-permute-done.2 = bf16[128,128]{1,0:T(8,128)(2,1)S(1)} collective-permute-done((bf16[128,128]{1,0:T(8,128)(2,1)S(1)}, bf16[128,128]{1,0:T(8,128)(2,1)S(1)}, u32[]{:S(2)}, u32[]{:S(2)}) %collective-permute-start.2) | collective-permute-done | bytes 32800 | tf_op jit(solution)/shard_map/ppermute | solution.py:36
  64.2 2.7 %collective-permute-start.3 = (bf16[128,128]{1,0:T(8,128)(2,1)S(1)}, bf16[128,128]{1,0:T(8,128)(2,1)S(1)}, u32[]{:S(2)}, u32[]{:S(2)}) collective-permute-start(bf16[128,128]{1,0:T(8,128)(2,1)S(1)} %fusion.16), channel_id=1, source_target_pairs={{0,1},{1,0},{2,3},{3,2},{4,5},{5,4},{6,7},{7,6},{8,9},{9,8},{10,11... | collective-permute-start | bytes 98312 | tf_op jit(solution)/shard_map/ppermute | solution.py:32
  66.9 0.9 collective-permute-done.3
  67.8 0.1 fusion.7
  67.9 0.1 copy.40
  68.0 0.0 copy-done
  68.1 0.3 convolution_convert_fusion
  68.4 16.7 %all_to_all.27 = bf16[16,8,2176]{2,1,0:T(8,128)(2,1)S(1)} all-to-all(bf16[16,8,2176]{2,1,0:T(8,128)(2,1)S(1)} %fusion.3), channel_id=1, replica_groups=mesh['kv'=16,'tp'=8] {'kv'}, dimensions={0} | all-to-all | bytes 1114112 | tf_op jit(solution)/shard_map/all_to_all | solution.py:227
  85.1 0.0 copy-start.1
  85.1 0.1 convert_reduce_fusion
  85.2 0.1 fusion.26
  85.3 0.1 fusion.14
  85.5 13.3 %all_to_all.28 = bf16[16,8,2048]{2,1,0:T(8,128)(2,1)S(1)} all-to-all(bf16[16,8,2048]{2,1,0:T(8,128)(2,1)S(1)} %broadcast_in_dim.54), channel_id=1, replica_groups=mesh['kv'=16,'tp'=8] {'kv'}, dimensions={0} | all-to-all | bytes 1048576 | tf_op jit(solution)/shard_map/all_to_all | solution.py:26
  98.8 0.0 copy-done.1
  98.8 0.3 fusion
  99.1 0.1 copy.41
  99.2 2.5 %collective-permute-start.4 = (bf16[4,32,128]{2,1,0:T(8,128)(2,1)S(1)}, bf16[4,32,128]{2,1,0:T(8,128)(2,1)S(1)}, u32[]{:S(2)}, u32[]{:S(2)}) collective-permute-start(bf16[4,32,128]{2,1,0:T(8,128)(2,1)S(1)} %fusion.19), channel_id=1, source_target_pairs={{0,1},{1,0},{2,3},{3,2},{4,5},{5,4},{6,7},{7,6},{8,9},{9,8},{10,11... | collective-permute-start | bytes 98312 | tf_op jit(solution)/shard_map/ppermute | solution.py:32
  101.7 0.9 collective-permute-done.4
  102.6 0.1 copy.46
  102.7 0.1 collective-permute-start.5
  102.8 0.1 copy.47
  103.0 3.0 %collective-permute-done.5 = bf16[2,32,128]{1,2,0:T(8,128)(2,1)S(1)} collective-permute-done((bf16[2,32,128]{1,2,0:T(8,128)(2,1)S(1)}, bf16[2,32,128]{1,2,0:T(8,128)(2,1)S(1)}, u32[]{:S(2)}, u32[]{:S(2)}) %collective-permute-start.5) | collective-permute-done | bytes 16416 | tf_op jit(solution)/shard_map/ppermute | solution.py:36
  106.0 1.0 collective-permute-start.6
  106.9 3.1 %collective-permute-done.6 = bf16[32,128]{0,1:T(8,128)(2,1)S(1)} collective-permute-done((bf16[32,128]{0,1:T(8,128)(2,1)S(1)}, bf16[32,128]{0,1:T(8,128)(2,1)S(1)}, u32[]{:S(2)}, u32[]{:S(2)}) %collective-permute-start.6) | collective-permute-done | bytes 8224 | tf_op jit(solution)/shard_map/ppermute | solution.py:36
  110.0 0.1 fusion.20
  110.1 0.7 copy.48
  (21 shorter events, 0.3 us)
Async XLA Ops:
  0.6 67.4 %copy-start = (bf16[256,2048]{1,0:T(8,128)(2,1)S(1)}, bf16[256,2048]{1,0:T(8,128)(2,1)}, u32[]{:S(2)}) copy-start(bf16[256,2048]{1,0:T(8,128)(2,1)} %param.19) | copy-start | bytes 3145732
  41.9 11.1 %all-to-all-start.2 = ((bf16[16,8,1024]{2,1,0:T(8,128)(2,1)}), bf16[16,8,1024]{2,1,0:T(8,128)(2,1)S(1)}, u32[]{:S(2)}, u32[]{:S(2)}) async-start(bf16[16,8,1024]{2,1,0:T(8,128)(2,1)} %get-tuple-element.16), calls=%async_computation.2 | async-start | bytes 524288 | tf_op jit(solution)/shard_map/all_to_all | solution.py:197
  45.5 7.5 %copy-start.2 = (bf16[1024,256]{1,0:T(8,128)(2,1)S(1)}, bf16[1024,256]{1,0:T(8,128)(2,1)}, u32[]{:S(2)}) copy-start(bf16[1024,256]{1,0:T(8,128)(2,1)} %param.18) | copy-start | bytes 1572868
  53.3 3.9 %collective-permute-start = (bf16[128,128]{1,0:T(8,128)(2,1)S(1)}, bf16[128,128]{1,0:T(8,128)(2,1)S(1)}, u32[]{:S(2)}, u32[]{:S(2)}) collective-permute-start(bf16[128,128]{1,0:T(8,128)(2,1)S(1)} %broadcast_select_fusion.2), channel_id=1, source_target_pairs={{0,1},{1,0},{2,3},{3,2},{4,5},{5,4},{6,7},{7,6},{8,9},{9,8},{10,11... | collective-permute-start | bytes 98312 | tf_op jit(solution)/shard_map/ppermute | solution.py:32
  57.3 2.8 %collective-permute-start.1 = (bf16[128,128]{1,0:T(8,128)(2,1)S(1)}, bf16[128,128]{1,0:T(8,128)(2,1)S(1)}, u32[]{:S(2)}, u32[]{:S(2)}) collective-permute-start(bf16[128,128]{1,0:T(8,128)(2,1)S(1)} %add_convert_fusion.1), channel_id=1, source_target_pairs={{0,2},{1,3},{2,0},{3,1},{4,6},{5,7},{6,4},{7,5},{8,10},{9,11},{10,... | collective-permute-start | bytes 98312 | tf_op jit(solution)/shard_map/ppermute | solution.py:36
  60.1 4.1 %collective-permute-start.2 = (bf16[128,128]{1,0:T(8,128)(2,1)S(1)}, bf16[128,128]{1,0:T(8,128)(2,1)S(1)}, u32[]{:S(2)}, u32[]{:S(2)}) collective-permute-start(bf16[128,128]{1,0:T(8,128)(2,1)S(1)} %add_convert_fusion), channel_id=1, source_target_pairs={{0,6},{1,7},{2,4},{3,5},{4,2},{5,3},{6,0},{7,1},{8,14},{9,15},{10,... | collective-permute-start | bytes 98312 | tf_op jit(solution)/shard_map/ppermute | solution.py:36
  64.2 3.6 %collective-permute-start.3 = (bf16[128,128]{1,0:T(8,128)(2,1)S(1)}, bf16[128,128]{1,0:T(8,128)(2,1)S(1)}, u32[]{:S(2)}, u32[]{:S(2)}) collective-permute-start(bf16[128,128]{1,0:T(8,128)(2,1)S(1)} %fusion.16), channel_id=1, source_target_pairs={{0,1},{1,0},{2,3},{3,2},{4,5},{5,4},{6,7},{7,6},{8,9},{9,8},{10,11... | collective-permute-start | bytes 98312 | tf_op jit(solution)/shard_map/ppermute | solution.py:32
  85.1 13.7 %copy-start.1 = (bf16[2048,256]{1,0:T(8,128)(2,1)S(1)}, bf16[2048,256]{1,0:T(8,128)(2,1)}, u32[]{:S(2)}) copy-start(bf16[2048,256]{1,0:T(8,128)(2,1)} %param.20) | copy-start | bytes 3145732
  99.2 3.3 %collective-permute-start.4 = (bf16[4,32,128]{2,1,0:T(8,128)(2,1)S(1)}, bf16[4,32,128]{2,1,0:T(8,128)(2,1)S(1)}, u32[]{:S(2)}, u32[]{:S(2)}) collective-permute-start(bf16[4,32,128]{2,1,0:T(8,128)(2,1)S(1)} %fusion.19), channel_id=1, source_target_pairs={{0,1},{1,0},{2,3},{3,2},{4,5},{5,4},{6,7},{7,6},{8,9},{9,8},{10,11... | collective-permute-start | bytes 98312 | tf_op jit(solution)/shard_map/ppermute | solution.py:32
  102.7 3.2 %collective-permute-start.5 = (bf16[2,32,128]{1,2,0:T(8,128)(2,1)S(1)}, bf16[2,32,128]{1,2,0:T(8,128)(2,1)S(1)}, u32[]{:S(2)}, u32[]{:S(2)}) collective-permute-start(bf16[2,32,128]{1,2,0:T(8,128)(2,1)S(1)} %copy.46), channel_id=1, source_target_pairs={{0,2},{1,3},{2,0},{3,1},{4,6},{5,7},{6,4},{7,5},{8,10},{9,11},{10,... | collective-permute-start | bytes 49160 | tf_op jit(solution)/shard_map/ppermute | solution.py:36
  106.0 4.1 %collective-permute-start.6 = (bf16[32,128]{0,1:T(8,128)(2,1)S(1)}, bf16[32,128]{0,1:T(8,128)(2,1)S(1)}, u32[]{:S(2)}, u32[]{:S(2)}) collective-permute-start(bf16[32,128]{0,1:T(8,128)(2,1)S(1)} %fusion.21), channel_id=1, source_target_pairs={{0,6},{1,7},{2,4},{3,5},{4,2},{5,3},{6,0},{7,1},{8,14},{9,15},{10,... | collective-permute-start | bytes 24584 | tf_op jit(solution)/shard_map/ppermute | solution.py:36

commit v3 on v2

--- a/solution.py
+++ b/solution.py
@@ -21,11 +21,23 @@
     return pltpu.with_memory_space_constraint(value, pltpu.HBM)
 
 
-def gather_all(value, axis):
-    size = lax.axis_size(axis)
-    return lax.all_to_all(
-        jnp.broadcast_to(value[None], (size, *value.shape)), axis, 0, 0, tiled=True
-    )
+def kernel(body, outs, in_specs, name, scratch=(), limit_mib=16, out_specs=None, flops=0):
+    return pl.pallas_call(
+        body,
+        out_shape=outs,
+        in_specs=in_specs,
+        out_specs=jax.tree.map(lambda _: VMEM, outs) if out_specs is None else out_specs,
+        scratch_shapes=list(scratch),
+        compiler_params=pltpu.CompilerParams(vmem_limit_bytes=limit_mib << 20),
+        cost_estimate=pl.CostEstimate(flops=flops, transcendentals=0, bytes_accessed=0)
+        if flops
+        else None,
+        name=name,
+    )
+
+
+def shape(dims, dtype):
+    return jax.ShapeDtypeStruct(dims, dtype)
 
 
 def swap_cores(value):
@@ -40,6 +52,25 @@
     lane = lax.broadcasted_iota(jnp.int32, (total.shape[0], width), 1)
     high = total.astype(BF16).astype(F32)
     return jnp.where(lane == 0, high, jnp.where(lane == 1, total - high, 0.0)).astype(BF16)
+
+
+def pack_body(where, act_hbm, mixer_hbm, channel_hbm, out, act_t, mixer, channel, sems):
+    pairs = ((act_hbm, act_t), (mixer_hbm, mixer), (channel_hbm, channel))
+    copies = [pltpu.make_async_copy(a, b, sems.at[i]) for i, (a, b) in enumerate(pairs)]
+    for copy in copies:
+        copy.start()
+    for copy in copies:
+        copy.wait()
+    first, slot = where[0] // 4, where[0] % 4
+    lane = lax.broadcasted_iota(jnp.int32, (8, 128), 1) // 32
+    row = lax.broadcasted_iota(jnp.int32, (8, 128), 0)
+    tiled = [jnp.concatenate([g[...].astype(F32)] * 4, axis=1) for g in (mixer, channel)]
+    gains = jnp.where(row == first, tiled[0], jnp.where(row == first + 2, tiled[1], 0.0))
+    gains = jnp.where(lane == slot, gains, 0.0).astype(BF16)
+    rows = act_t[...]
+    for j in range(8):
+        out[j, :32, :] = rows
+        out[j, 32:, :] = gains
 
 
 def project_body(packed, wq, wk, wv, wg, terms, stream_out, gains_out, bq, bk, bv, bg, sems):
@@ -75,6 +106,7 @@
     query_t = query.T
     key_out[...] = key.T
     value_out[...] = value
+    silu = gate * jax.nn.sigmoid(gate)
     for b in range(8):
         copies[b].wait()
         for h in range(2):
@@ -89,10 +121,24 @@
         match = jnp.sum(query[:, heads] * key[:, heads], axis=1, keepdims=True)
         out = rates[h] * kept[:, cols] + match * value[:, cols]
         out = out * lax.rsqrt(jnp.mean(out * out, axis=1, keepdims=True) + EPS)
-        g = gate[:, cols]
-        mixed = (g * jax.nn.sigmoid(g) * out).astype(BF16)
+        mixed = (silu[:, cols] * out).astype(BF16)
         for j in range(16):
             mixed_out[j, :, cols] = mixed
+
+
+def lift_body(parts, out):
+    sums = jnp.sum(parts[...].astype(F32), axis=0)
+    scale = lax.rsqrt((sums[:, 2048:2049] + sums[:, 2049:2050]) / D + EPS)
+    lifted = jnp.maximum(scale * sums[:, :2048], 0.0)
+    hidden = (lifted * lifted).astype(BF16)
+    for j in range(16):
+        out[j] = hidden
+
+
+def finish_body(where, parts, middle_t, out):
+    lowered = jnp.sum(parts[...].astype(F32), axis=0)
+    own = middle_t[pl.ds(pl.multiple_of(where[0] * 32, 32), 32), :]
+    out[...] = (own.astype(F32) + lowered).astype(BF16)
 
 
 def advance_body(rates, key_t, value, state_hbm, new_hbm, state, new, in_sems, out_sems):
@@ -127,56 +173,43 @@
 ):
     tp = lax.axis_index("tp")
     core = tp % 2
-    chip = tp // 2
     heads_dev = state_in.shape[1]
     index = (tp * heads_dev + jnp.arange(heads_dev, dtype=jnp.int32)).astype(F32)
     rates = 1.0 - 2.0 ** (-1.0 - 6.0 * index / (HEADS - 1))
 
-    spread = jnp.arange(128) // 32 == tp % 4
-    tiled = [jnp.where(spread, jnp.tile(g, 4), 0) for g in (mixer_gain, channel_gain)]
-    row = jnp.arange(8)[:, None]
-    first = tp // 4
-    gain_rows = jnp.where(row == first, tiled[0], jnp.where(row == first + 2, tiled[1], 0))
-    rows = jnp.concatenate([activations.T, gain_rows.astype(BF16)], axis=0)
-    rows, rates = lax.optimization_barrier((rows, rates))
-    packed = gather_all(rows, "tp")
-
+    where = tp.astype(jnp.int32)[None]
+    where, rates = lax.optimization_barrier((where, rates))
+    sources = (activations.T, mixer_gain[None], channel_gain[None])
+    rows = kernel(
+        pack_body,
+        shape((8, 40, 128), BF16),
+        [SMEM, HBM, HBM, HBM],
+        "pack",
+        [pltpu.VMEM(v.shape, BF16) for v in sources] + [pltpu.SemaphoreType.DMA((3,))],
+    )(where, *map(in_hbm, sources))
+    packed = lax.all_to_all(rows, "tp", 0, 0, tiled=True)
     weights = (query_weight, key_weight, value_weight, gate_weight)
-    terms, stream, gains = pl.pallas_call(
+    terms, stream, gains = kernel(
         project_body,
-        out_shape=(
-            jax.ShapeDtypeStruct((128, 3200), BF16),
-            jax.ShapeDtypeStruct((128, 256), BF16),
-            jax.ShapeDtypeStruct((8, 128), F32),
-        ),
-        in_specs=[VMEM, HBM, HBM, HBM, HBM],
-        out_specs=(VMEM, VMEM, VMEM),
-        scratch_shapes=[pltpu.VMEM(w.shape, BF16) for w in weights]
-        + [pltpu.SemaphoreType.DMA((4,))],
-        compiler_params=pltpu.CompilerParams(vmem_limit_bytes=16 << 20),
-        name="project",
+        (shape((128, 3200), BF16), shape((128, 256), BF16), shape((8, 128), F32)),
+        [VMEM, HBM, HBM, HBM, HBM],
+        "project",
+        [pltpu.VMEM(w.shape, BF16) for w in weights] + [pltpu.SemaphoreType.DMA((4,))],
     )(packed, *map(in_hbm, weights))
     channel = jnp.concatenate([gains[2:3], gains[3:4]], axis=1)
     stream = stream.astype(F32)
     parts = lax.all_to_all(terms.reshape(16, 8, 3200), "kv", 0, 0, tiled=True)
-
     state = in_hbm(state_in)
-    mixed, key_t, value = pl.pallas_call(
+    mixed, key_t, value = kernel(
         retain_body,
-        out_shape=(
-            jax.ShapeDtypeStruct((16, 8, 1024), BF16),
-            jax.ShapeDtypeStruct((512, 8), F32),
-            jax.ShapeDtypeStruct((8, 1024), F32),
-        ),
-        in_specs=[SMEM, VMEM, HBM],
-        out_specs=(VMEM, VMEM, VMEM),
-        scratch_shapes=[
+        (shape((16, 8, 1024), BF16), shape((512, 8), F32), shape((8, 1024), F32)),
+        [SMEM, VMEM, HBM],
+        "retain",
+        [
             pltpu.VMEM((8, 1024), F32),
             pltpu.VMEM(state_in.shape, F32),
             pltpu.SemaphoreType.DMA((8,)),
         ],
-        compiler_params=pltpu.CompilerParams(vmem_limit_bytes=16 << 20),
-        name="retain",
     )(rates, parts, state)
     new_state = pl.pallas_call(
         advance_body,
@@ -220,27 +253,20 @@
     up_terms = jnp.concatenate(
         [
             jnp.dot(channel_normed, up_weight, preferred_element_type=F32).astype(BF16),
-            jnp.pad(middle_squares.astype(BF16), ((0, 0), (0, 127))),
+            squares_lanes(middle_squares, 128),
         ],
         axis=1,
     )
+    up_terms, middle_t = lax.optimization_barrier((up_terms, middle_bf.T))
     up_parts = lax.all_to_all(up_terms.reshape(16, 8, -1), "kv", 0, 0, tiled=True)
-    up_sum = jnp.sum(up_parts.astype(F32), axis=0)
-    lifted = lax.rsqrt(up_sum[:, 2048:2049] / D + EPS) * up_sum[:, :2048]
-    hidden = jnp.square(jax.nn.relu(lifted)).astype(BF16)
-
-    hidden_all = gather_all(hidden, "kv").reshape(128, 2048)
+    hidden = kernel(lift_body, shape((16, 8, 2048), BF16), [VMEM], "lift")(up_parts)
+    hidden_all = lax.all_to_all(hidden, "kv", 0, 0, tiled=True).reshape(128, 2048)
     down_terms = jnp.dot(hidden_all, down_weight, preferred_element_type=F32).astype(BF16)
-    down_t = down_terms.T.reshape(4, 2, 32, 128)
-    mine = jnp.where(core == 0, down_t[:, 0], down_t[:, 1])
-    theirs = jnp.where(core == 0, down_t[:, 1], down_t[:, 0])
-    pair = (mine.astype(F32) + swap_cores(theirs).astype(F32)).astype(BF16)
-    keep = jnp.stack([lax.dynamic_index_in_dim(pair, chip ^ m, 0, keepdims=False) for m in (0, 3)])
-    give = jnp.stack([lax.dynamic_index_in_dim(pair, chip ^ m, 0, keepdims=False) for m in (1, 2)])
-    keep = keep.astype(F32) + swap_chips(give, 1).astype(F32)
-    lowered = keep[0] + swap_chips(keep[1].astype(BF16), 3).astype(F32)
-    own = lax.dynamic_slice_in_dim(middle_bf.T, tp * 32, 32, 0).astype(F32)
-    return ((own + lowered).astype(BF16).T, new_state)
+    down_parts = lax.all_to_all(down_terms.T.reshape(8, 32, 128), "tp", 0, 0, tiled=True)
+    out_t = kernel(finish_body, shape((32, 128), BF16), [SMEM, VMEM, VMEM], "finish")(
+        where, down_parts, middle_t
+    )
+    return (out_t.T, new_state)
 
 
 def solution(mesh):

time: 113 us -> 108 us (0.956); the launches traced: 111 us -> 108 us
  blocking collectives: 61.8 us -> 71.6 us
  waiting for transfers between devices: 14.2 us -> 7.16 us
  starting transfers between devices: 14.2 us -> 10.7 us
  local copies, waits for them, and re-layouts: 2.82 us -> 0.24 us
  Pallas kernels: 14.5 us -> 16.1 us
  other arithmetic: 1.46 us -> 0.31 us
    all_to_all x2 -> x3, blocking collectives: 23.8 us -> 33.6 us  [the longest x1 13.5 us: per_device(): lax.all_to_all(hidden, 'kv', 0, 0, tiled=True).reshape(128, 2048)]
    ppermute x4 -> x2, waiting for transfers between devices: 11.6 us -> 5.42 us  [swap_chips(): return lax.ppermute(value, 'tp', [(i, i ^ 2 * mask) for i in range(8)])]
    ppermute x3 -> x2, starting transfers between devices: 8.28 us -> 5.83 us  [swap_cores(): return lax.ppermute(value, 'tp', [(i, i ^ 1) for i in range(8)])]
    another operation x5 -> x0, local copies, waits for them, and re-layouts: 1.69 us -> none  [the longest x4 1.57 us: per_device(): jnp.tile(g, 4)]
    pallas_call x2 -> x5, Pallas kernels: 7.03 us -> 8.58 us  [the longest x1 5.03 us: per_device(): kernel(retain_body, (shape((16, 8, 1024), BF16), shape((512, 8), F32), sh...]
    ppermute x4 -> x2, starting transfers between devices: 2.38 us -> 1.33 us  [swap_chips(): return lax.ppermute(value, 'tp', [(i, i ^ 2 * mask) for i in range(8)])]
    ppermute x3 -> x2, waiting for transfers between devices: 2.58 us -> 1.72 us  [swap_cores(): return lax.ppermute(value, 'tp', [(i, i ^ 1) for i in range(8)])]
  transfers between devices with their start and end apart: 8 -> 5, of which waited for: 7 -> 4; matrix products, arithmetic and copies ran while one was open for 0% -> 0% of each run, Pallas kernels for 7% -> 7%
where the time goes in v3:
time: 108 us
  blocking collectives  71.6 us (66%)
  Pallas kernels  16.1 us (15%)
  starting transfers between devices  10.7 us (10%)
  waiting for transfers between devices  7.16 us (7%)
  matrix products  1.08 us (1%)
    all_to_all x1, blocking collectives, per_device(): parts = lax.all_to_all(terms.reshape(16, 8, 3200), 'kv', 0, 0, tiled=True)  21.3 us
    all_to_all x1, blocking collectives, per_device(): lax.all_to_all(up_terms.reshape(16, 8, -1), 'kv', 0, 0, tiled=True)  16.7 us
    all_to_all x1, blocking collectives, per_device(): lax.all_to_all(hidden, 'kv', 0, 0, tiled=True).reshape(128, 2048)  13.5 us
    all_to_all x1, blocking collectives, per_device(): packed = lax.all_to_all(rows, 'tp', 0, 0, tiled=True)  10.5 us
    all_to_all x1, blocking collectives, per_device(): lax.all_to_all(down_terms.T.reshape(8, 32, 128), 'tp', 0, 0, tiled=True)  9.61 us
    pallas_call x1, Pallas kernels, per_device(): pl.pallas_call(advance_body, out_shape=jax.ShapeDtypeStruct(state_in.shap...  7.47 us
    ppermute x2, starting transfers between devices, swap_cores(): return lax.ppermute(value, 'tp', [(i, i ^ 1) for i in range(8)])  5.83 us
    ppermute x2, waiting for transfers between devices, swap_chips(): return lax.ppermute(value, 'tp', [(i, i ^ 2 * mask) for i in range(8)])  5.42 us
  transfers between devices with their start and end apart: 5, of which 4 were waited for; matrix products, arithmetic and copies ran while one was open for 0% of the time, Pallas kernels for 7%

profile of v3, /device:TPU:1, one launch (start us, length us, event | category | flops | bytes accessed | tf_op | source)
XLA Modules:
  0.0 107.9 jit_solution(13428346468493856354)
XLA Ops:
  0.6 0.0 copy-start
  0.7 0.9 pack.1
  1.6 10.5 %all_to_all.30.packed = bf16[8,40,128]{2,1,0:T(8,128)(2,1)S(1)} all-to-all(bf16[8,40,128]{2,1,0:T(8,128)(2,1)S(1)} %pack.1), channel_id=1, replica_groups=mesh['kv'=16,'tp'=8] {'tp'}, dimensions={0} | all-to-all | bytes 163840 | tf_op jit(solution)/shard_map/all_to_all | solution.py:190
  12.1 1.8 %project.1 = (bf16[128,3200]{1,0:T(8,128)(2,1)S(1)}, bf16[128,256]{1,0:T(8,128)(2,1)S(1)}, f32[8,128]{1,0:T(8,128)S(1)}) custom-call(bf16[8,40,128]{2,1,0:T(8,128)(2,1)S(1)} %all_to_all.30.packed, bf16[256,512]{1,0:T(8,128)(2,1)} %wq.1, bf16[256,512]{1,0:T(8,128)(2,1)} %wk.1, bf16[256,1024]{1,0:T(8,128)(2,1)} %wv.1, bf16[256,1024]{1,0:T(8,128)(2,1)} %wg.1), custom_call_target="tpu_custom_call" | custom-call | tf_op jit(solution)/shard_map/project/pallas_call | solution.py:192
  13.9 21.3 %all_to_all.31.parts = bf16[16,8,3200]{2,1,0:T(8,128)(2,1)S(1)} all-to-all(bf16[16,8,3200]{2,1,0:T(8,128)(2,1)S(1)} %bitcast.22), channel_id=1, replica_groups=mesh['kv'=16,'tp'=8] {'kv'}, dimensions={0} | all-to-all | bytes 1638400 | tf_op jit(solution)/shard_map/all_to_all | solution.py:201
  35.2 5.0 %retain.1 = (bf16[16,8,1024]{2,1,0:T(8,128)(2,1)}, f32[512,8]{1,0:T(8,128)S(1)}, f32[8,1024]{1,0:T(8,128)S(1)}) custom-call(f32[2]{0:T(128)S(1)} %power_subtract_fusion.rates, bf16[16,8,3200]{2,1,0:T(8,128)(2,1)S(1)} %all_to_all.31.parts, f32[8,2,256,512]{3,2,1,0:T(8,128)} %state_hbm.3), custom_call_target="tpu_custom_call" | custom-call | tf_op jit(solution)/shard_map/retain/pallas_call | solution.py:203
  40.3 3.5 %all-to-all-start.2 = ((bf16[16,8,1024]{2,1,0:T(8,128)(2,1)}), bf16[16,8,1024]{2,1,0:T(8,128)(2,1)S(1)}, u32[]{:S(2)}, u32[]{:S(2)}) async-start(bf16[16,8,1024]{2,1,0:T(8,128)(2,1)} %get-tuple-element.18), calls=%async_computation.2 | async-start | bytes 524288 | tf_op jit(solution)/shard_map/all_to_all | solution.py:230
  43.8 0.0 copy-start.2
  43.9 7.5 %advance.1 = f32[8,2,256,512]{3,2,1,0:T(8,128)} custom-call(f32[2]{0:T(128)S(1)} %power_subtract_fusion.rates, f32[512,8]{1,0:T(8,128)S(1)} %get-tuple-element.19.key_t, f32[8,1024]{1,0:T(8,128)S(1)} %get-tuple-element.20.value, f32[8,2,256,512]{3,2,1,0:T(8,128)} %state_hbm.3), custom_call_target="tpu_custom_call" | custom-call | flops 40000000 | bytes 16777216 | tf_op jit(solution)/shard_map/advance/pallas_call | solution.py:214
  51.3 0.0 all-to-all-done.2
  51.4 0.0 copy-done.2
  51.4 0.3 convolution_convert_fusion.2
  51.7 3.1 %collective-permute-start = (bf16[128,128]{0,1:T(8,128)(2,1)S(1)}, bf16[128,128]{0,1:T(8,128)(2,1)S(1)}, u32[]{:S(2)}, u32[]{:S(2)}) collective-permute-start(bf16[128,128]{0,1:T(8,128)(2,1)S(1)} %broadcast_select_fusion.2), channel_id=1, source_target_pairs={{0,1},{1,0},{2,3},{3,2},{4,5},{5,4},{6,7},{7,6},{8,9},{9,8},{10,11... | collective-permute-start | bytes 98312 | tf_op jit(solution)/shard_map/ppermute | solution.py:44
  54.8 0.9 collective-permute-done
  55.7 0.4 collective-permute-start.1
  56.1 2.5 %collective-permute-done.1 = bf16[128,128]{0,1:T(8,128)(2,1)S(1)} collective-permute-done((bf16[128,128]{0,1:T(8,128)(2,1)S(1)}, bf16[128,128]{0,1:T(8,128)(2,1)S(1)}, u32[]{:S(2)}, u32[]{:S(2)}) %collective-permute-start.1) | collective-permute-done | bytes 32800 | tf_op jit(solution)/shard_map/ppermute | solution.py:48
  58.6 1.0 collective-permute-start.2
  59.5 0.1 copy.13
  59.7 2.9 %collective-permute-done.2 = bf16[128,128]{0,1:T(8,128)(2,1)S(1)} collective-permute-done((bf16[128,128]{0,1:T(8,128)(2,1)S(1)}, bf16[128,128]{0,1:T(8,128)(2,1)S(1)}, u32[]{:S(2)}, u32[]{:S(2)}) %collective-permute-start.2) | collective-permute-done | bytes 32800 | tf_op jit(solution)/shard_map/ppermute | solution.py:48
  62.7 2.7 %collective-permute-start.3 = (bf16[128,128]{0,1:T(8,128)(2,1)S(1)}, bf16[128,128]{0,1:T(8,128)(2,1)S(1)}, u32[]{:S(2)}, u32[]{:S(2)}) collective-permute-start(bf16[128,128]{0,1:T(8,128)(2,1)S(1)} %fusion.7), channel_id=1, source_target_pairs={{0,1},{1,0},{2,3},{3,2},{4,5},{5,4},{6,7},{7,6},{8,9},{9,8},{10,11... | collective-permute-start | bytes 98312 | tf_op jit(solution)/shard_map/ppermute | solution.py:44
  65.4 0.9 collective-permute-done.3
  66.3 0.1 fusion.4
  66.3 0.0 copy-done
  66.3 0.4 convolution_convert_fusion
  66.8 0.1 select_convert_fusion
  66.9 16.7 %all_to_all.32.parts = bf16[16,8,2176]{2,1,0:T(8,128)(2,1)S(1)} all-to-all(bf16[16,8,2176]{2,1,0:T(8,128)(2,1)S(1)} %bitcast.23), channel_id=1, replica_groups=mesh['kv'=16,'tp'=8] {'kv'}, dimensions={0} | all-to-all | bytes 1114112 | tf_op jit(solution)/shard_map/all_to_all | solution.py:261
  83.6 0.0 copy-start.1
  83.6 0.2 lift.1
  83.8 13.5 %all_to_all.33 = bf16[16,8,2048]{2,1,0:T(8,128)(2,1)S(1)} all-to-all(bf16[16,8,2048]{2,1,0:T(8,128)(2,1)S(1)} %lift.1), channel_id=1, replica_groups=mesh['kv'=16,'tp'=8] {'kv'}, dimensions={0} | all-to-all | bytes 1048576 | tf_op jit(solution)/shard_map/all_to_all | solution.py:263
  97.3 0.0 copy-done.1
  97.3 0.3 fusion
  97.6 0.1 copy.15
  97.7 9.6 %all_to_all.34.parts = bf16[8,32,128]{2,1,0:T(8,128)(2,1)S(1)} all-to-all(bf16[8,32,128]{2,1,0:T(8,128)(2,1)S(1)} %bitcast.24), channel_id=1, replica_groups=mesh['kv'=16,'tp'=8] {'tp'}, dimensions={0} | all-to-all | bytes 131072 | tf_op jit(solution)/shard_map/all_to_all | solution.py:265
  107.3 0.6 finish.1
  (14 shorter events, 0.2 us)
Async XLA Ops:
  0.6 65.7 %copy-start = (bf16[256,2048]{1,0:T(8,128)(2,1)S(1)}, bf16[256,2048]{1,0:T(8,128)(2,1)}, u32[]{:S(2)}) copy-start(bf16[256,2048]{1,0:T(8,128)(2,1)} %param.19) | copy-start | bytes 3145732
  40.3 11.1 %all-to-all-start.2 = ((bf16[16,8,1024]{2,1,0:T(8,128)(2,1)}), bf16[16,8,1024]{2,1,0:T(8,128)(2,1)S(1)}, u32[]{:S(2)}, u32[]{:S(2)}) async-start(bf16[16,8,1024]{2,1,0:T(8,128)(2,1)} %get-tuple-element.18), calls=%async_computation.2 | async-start | bytes 524288 | tf_op jit(solution)/shard_map/all_to_all | solution.py:230
  43.8 7.5 %copy-start.2 = (bf16[1024,256]{1,0:T(8,128)(2,1)S(1)}, bf16[1024,256]{1,0:T(8,128)(2,1)}, u32[]{:S(2)}) copy-start(bf16[1024,256]{1,0:T(8,128)(2,1)} %param.18) | copy-start | bytes 1572868
  51.7 4.0 %collective-permute-start = (bf16[128,128]{0,1:T(8,128)(2,1)S(1)}, bf16[128,128]{0,1:T(8,128)(2,1)S(1)}, u32[]{:S(2)}, u32[]{:S(2)}) collective-permute-start(bf16[128,128]{0,1:T(8,128)(2,1)S(1)} %broadcast_select_fusion.2), channel_id=1, source_target_pairs={{0,1},{1,0},{2,3},{3,2},{4,5},{5,4},{6,7},{7,6},{8,9},{9,8},{10,11... | collective-permute-start | bytes 98312 | tf_op jit(solution)/shard_map/ppermute | solution.py:44
  55.7 2.8 %collective-permute-start.1 = (bf16[128,128]{0,1:T(8,128)(2,1)S(1)}, bf16[128,128]{0,1:T(8,128)(2,1)S(1)}, u32[]{:S(2)}, u32[]{:S(2)}) collective-permute-start(bf16[128,128]{0,1:T(8,128)(2,1)S(1)} %add_convert_fusion.1), channel_id=1, source_target_pairs={{0,2},{1,3},{2,0},{3,1},{4,6},{5,7},{6,4},{7,5},{8,10},{9,11},{10,... | collective-permute-start | bytes 98312 | tf_op jit(solution)/shard_map/ppermute | solution.py:48
  58.6 4.1 %collective-permute-start.2 = (bf16[128,128]{0,1:T(8,128)(2,1)S(1)}, bf16[128,128]{0,1:T(8,128)(2,1)S(1)}, u32[]{:S(2)}, u32[]{:S(2)}) collective-permute-start(bf16[128,128]{0,1:T(8,128)(2,1)S(1)} %add_convert_fusion), channel_id=1, source_target_pairs={{0,6},{1,7},{2,4},{3,5},{4,2},{5,3},{6,0},{7,1},{8,14},{9,15},{10,... | collective-permute-start | bytes 98312 | tf_op jit(solution)/shard_map/ppermute | solution.py:48
  62.7 3.6 %collective-permute-start.3 = (bf16[128,128]{0,1:T(8,128)(2,1)S(1)}, bf16[128,128]{0,1:T(8,128)(2,1)S(1)}, u32[]{:S(2)}, u32[]{:S(2)}) collective-permute-start(bf16[128,128]{0,1:T(8,128)(2,1)S(1)} %fusion.7), channel_id=1, source_target_pairs={{0,1},{1,0},{2,3},{3,2},{4,5},{5,4},{6,7},{7,6},{8,9},{9,8},{10,11... | collective-permute-start | bytes 98312 | tf_op jit(solution)/shard_map/ppermute | solution.py:44
  83.6 13.7 %copy-start.1 = (bf16[2048,256]{1,0:T(8,128)(2,1)S(1)}, bf16[2048,256]{1,0:T(8,128)(2,1)}, u32[]{:S(2)}) copy-start(bf16[2048,256]{1,0:T(8,128)(2,1)} %param.20) | copy-start | bytes 3145732
